TPU v7x, 512 devices: a whole 4x8x8 slice. The times are simulated.
512 devices in a mesh: fs: 64 (over z, y), tp: 8 (over x, core).
Axes of the slice: x: 4, y: 8, z: 8, core: 2. Of those that a mesh axis runs over, the one named last changes fastest.
Arguments:
- normed: bfloat16 [65536, 2048], P('fs'), may hold values from -6 to 6
- key_cot: bfloat16 [65536, 1024], P('fs', 'tp'), may hold values from -130 to 130
- value_cot: bfloat16 [65536, 2048], P('fs', 'tp'), may hold values from -130 to 130
- basis: bfloat16 [2048, 256], P('fs'), may hold values from -3.535534 to 3.535534
- master_key: float32 [2048, 1024], P('fs', 'tp'), may hold values from -3 to 3
- master_value: float32 [2048, 2048], P('fs', 'tp'), may hold values from -3 to 3
- first_key: float32 [256, 1024], P('fs', 'tp'), may hold values from -3 to 3
- second_key: float32 [256, 1024], P('fs', 'tp'), may hold values from 0.05 to 2
- first_value: float32 [256, 2048], P('fs', 'tp'), may hold values from -3 to 3
- second_value: float32 [256, 2048], P('fs', 'tp'), may hold values from 0.05 to 2
Outputs:
- step_key: float32 [2048, 1024], P('fs', 'tp')
- step_value: float32 [2048, 2048], P('fs', 'tp')
- new_master_key: float32 [2048, 1024], P('fs', 'tp')
- new_master_value: float32 [2048, 2048], P('fs', 'tp')
- copy_key: bfloat16 [2048, 1024], P(None, 'tp')
- copy_value: bfloat16 [2048, 2048], P(None, 'tp')
- new_first_key: float32 [256, 1024], P('fs', 'tp')
- new_second_key: float32 [256, 1024], P('fs', 'tp')
- new_first_value: float32 [256, 2048], P('fs', 'tp')
- new_second_value: float32 [256, 2048], P('fs', 'tp')
All inputs are finite; a program needn't handle non-finite values.
Results may differ from a plain program's by a relative error of at most 0.0055.
Values may be sent and summed in bfloat16 or wider, within the bound.
A program may use at most 64 MiB of HBM per device.

v0:
```python
import functools

import jax
import jax.numpy as jnp
from jax import lax
from jax.experimental import pallas as pl
from jax.experimental.pallas import tpu as pltpu
from jax.sharding import PartitionSpec as P

learn_rate = 0.05
beta_first = 0.9
beta_second = 0.9
epsilon = 1e-08
norm_eps = 1e-06

SHARES = (16, 16, 16)

MESH = pl.DeviceIdType.MESH
F32 = jnp.float32
BF16 = jnp.bfloat16


class Gather:
    def __init__(self, lines, slot, own, send_sem, recv_sem):
        self.lines, self.slot, self.own = lines, slot, own
        self.send_sem, self.recv_sem = send_sem, recv_sem
        self.me = lax.axis_index("fs")
        self.z = self.me // 4
        self.y = lax.rem(self.me // 2, 2)
        self.x = lax.rem(self.me, 2)
        self.along = [self.partner(i) for i in range(lines)]
        self.sent = []

    def partner(self, i):
        out, bit = self.z, 1
        while bit <= i:
            if i & bit:
                out = out + bit - 2 * bit * lax.rem(self.z // bit, 2)
            bit *= 2
        return out

    def at(self, i, fy, fx):
        y = 1 - self.y if fy else self.y
        x = 1 - self.x if fx else self.x
        return self.along[i] * 4 + y * 2 + x

    def send(self, part, index, source, owner, target):
        copy = pltpu.make_async_remote_copy(
            src_ref=source,
            dst_ref=self.slot(owner, part),
            send_sem=self.send_sem.at[part, index],
            recv_sem=self.recv_sem.at[part, index],
            device_id={"fs": target},
            device_id_type=MESH,
        )
        copy.start()
        self.sent.append(copy)

    def arrive(self, part, index, owner):
        place = self.slot(owner, part)
        pltpu.make_async_remote_copy(
            src_ref=place,
            dst_ref=place,
            send_sem=self.send_sem.at[part, index],
            recv_sem=self.recv_sem.at[part, index],
            device_id={"fs": self.at(0, 0, 1)},
            device_id_type=MESH,
        ).wait_recv()

    def flips(self, part):
        return ((1, 0), (0, 1)) if part == 0 else ((0, 1), (1, 0))

    def along_z(self, start=1, stop=None):
        for k in range(start, stop or self.lines):
            for part in range(2):
                self.send(part, k, self.own(part), self.me, self.at(k, 0, 0))

    def hop_one(self, part, i):
        first, _ = self.flips(part)
        owner = self.at(i, 0, 0)
        source = self.own(part) if i == 0 else self.slot(owner, part)
        self.send(part, self.lines + i, source, owner, self.at(0, *first))

    def hop_two(self, part, i, flipped):
        first, second = self.flips(part)
        owner = self.at(i, *first) if flipped else self.at(i, 0, 0)
        source = self.own(part) if i == 0 and not flipped else self.slot(owner, part)
        self.send(part, (3 if flipped else 2) * self.lines + i, source, owner, self.at(0, *second))

    def steps(self):
        def begin():
            for part in range(2):
                self.hop_one(part, 0)
            for part in range(2):
                self.hop_two(part, 0, False)

        def from_line(i):
            for part in range(2):
                self.arrive(part, i, self.at(i, 0, 0))
                self.hop_one(part, i)
            for part in range(2):
                self.hop_two(part, i, False)

        def from_first(i):
            for part in range(2):
                first, _ = self.flips(part)
                self.arrive(part, self.lines + i, self.at(i, *first))
                self.hop_two(part, i, True)

        def from_second(i):
            for part in range(2):
                first, second = self.flips(part)
                self.arrive(part, 2 * self.lines + i, self.at(i, *second))
                self.arrive(part, 3 * self.lines + i, self.at(i, 1, 1))

        out = [begin]
        for i in range(1, self.lines):
            out.append(functools.partial(from_line, i))
            out.append(functools.partial(from_first, i - 1))
        out.append(functools.partial(from_first, self.lines - 1))
        tail = [functools.partial(from_second, i) for i in range(self.lines)]
        return out, tail

    def close(self):
        for copy in self.sent:
            copy.wait_send()


def exchange_kernel(
    n,
    tp,
    count,
    normed,
    key_cot,
    value_cot,
    basis_in,
    master_key,
    master_value,
    first_key_in,
    second_key_in,
    first_value_in,
    second_value_in,
    basis_all,
    master_all,
    dirs_all,
    scaled_out,
    normed_v,
    key_v,
    value_v,
    basis,
    master_key_v,
    master_value_v,
    first_key,
    second_key,
    first_value,
    second_value,
    master,
    projected,
    partial,
    received,
    direction,
    own_square,
    squares,
    chip_square,
    chip_squares,
    load_sem,
    basis_send,
    basis_recv,
    master_send,
    master_recv,
    dirs_send,
    dirs_recv,
    part_send,
    part_recv,
    square_send,
    square_recv,
    chip_send,
    chip_recv,
):
    me = lax.axis_index("fs")
    my_tp = lax.axis_index("tp")
    loads = [
        pltpu.make_async_copy(source, target, load_sem.at[i])
        for i, (source, target) in enumerate(
            (
                (basis_in, basis),
                (master_key, master_key_v),
                (master_value, master_value_v),
                (normed, normed_v),
                (key_cot, key_v),
                (value_cot, value_v),
                (first_key_in, first_key),
                (second_key_in, second_key),
                (first_value_in, first_value),
                (second_value_in, second_value),
            )
        )
    ]
    for load in loads:
        load.start()

    barrier = pltpu.get_barrier_semaphore()
    for k in range(1, n):
        pl.semaphore_signal(barrier, inc=1, device_id={"fs": lax.rem(me + k, n)}, device_id_type=MESH)
    for k in range(1, tp):
        pl.semaphore_signal(barrier, inc=1, device_id={"tp": lax.rem(my_tp + k, tp)}, device_id_type=MESH)
    pl.semaphore_wait(barrier, n - 1 + tp - 1)

    lines = n // 4

    def gather(whole, own, send_sem, recv_sem, stacked):
        cols = own.shape[-1]
        cut = cols // 256 * 128
        spans = (pl.ds(0, cut), pl.ds(cut, cols - cut))
        rows = own.shape[0]

        def slot(owner, part):
            if stacked:
                return whole.at[owner, :, spans[part]]
            return whole.at[pl.ds(pl.multiple_of(owner * rows, rows), rows), spans[part]]

        return Gather(lines, slot, lambda part: own.at[:, spans[part]], send_sem, recv_sem)

    basis_g = gather(basis_all, basis, basis_send, basis_recv, False)
    master_g = gather(master_all, master, master_send, master_recv, False)
    dirs_g = gather(dirs_all, direction, dirs_send, dirs_recv, True)

    loads[0].wait()
    basis_g.along_z()
    steps, tail = basis_g.steps()
    steps[0]()
    loads[1].wait()
    loads[2].wait()
    cut = master_key_v.shape[1]
    master[:, :cut] = master_key_v[...].astype(BF16)
    master[:, cut:] = master_value_v[...].astype(BF16)
    early = lines
    master_g.along_z(1, early)
    rows = basis.shape[0]
    own_rows = pl.ds(pl.multiple_of(me * rows, rows), rows)
    basis_all[own_rows, :] = basis[...]
    master_all[own_rows, :] = master[...]
    for step in steps[1:]:
        step()
    master_steps, master_tail = master_g.steps()
    master_steps[0]()
    for step in tail:
        step()

    loads[3].wait()
    tokens = normed_v.shape[0]
    tile = 256

    @pl.loop(0, tokens // tile)
    def _(t):
        at = pl.ds(pl.multiple_of(t * tile, tile), tile)
        projected[at, :] = jnp.dot(normed_v[at, :], basis_all[...], preferred_element_type=F32).astype(BF16)

    loads[4].wait()
    loads[5].wait()
    kc = key_v.shape[1]
    rank_rows = first_key.shape[0]

    def project(cot, base):
        width = cot.shape[1]
        step = min(width, 512)
        for c in range(0, width, step):
            sums = lax.dot_general(
                projected[...], cot[:, c : c + step], (((0,), (0,)), ((), ())), preferred_element_type=F32
            ).astype(BF16)
            for j in range(n):
                partial[j, :, base + c : base + c + step] = sums[j * rank_rows : (j + 1) * rank_rows, :]

    project(key_v, 0)
    project(value_v, kc)

    part_copies = []
    for k in range(1, n):
        target = lax.rem(me + k, n)
        copy = pltpu.make_async_remote_copy(
            src_ref=partial.at[target],
            dst_ref=received.at[k],
            send_sem=part_send.at[k],
            recv_sem=part_recv.at[k],
            device_id={"fs": target},
            device_id_type=MESH,
        )
        copy.start()
        part_copies.append(copy)
    low = partial[me].astype(F32)
    received[0] = partial[me]
    master_g.along_z(early, lines)
    turns = [len(master_steps) * part // 16 for part in SHARES]
    for step in master_steps[1 : turns[0]]:
        step()
    for k, copy in enumerate(part_copies):
        copy.wait_recv()
    low = received[0].astype(F32)
    for k in range(1, n):
        low = low + received[k].astype(F32)

    square = jnp.sum(low * low)
    own_square[...] = jnp.full(own_square.shape, square, F32)
    squares[0] = jnp.full(own_square.shape, square, F32)
    square_copies = []
    for k in range(1, n):
        copy = pltpu.make_async_remote_copy(
            src_ref=own_square,
            dst_ref=squares.at[k],
            send_sem=square_send.at[k],
            recv_sem=square_recv.at[k],
            device_id={"fs": lax.rem(me + k, n)},
            device_id_type=MESH,
        )
        copy.start()
        square_copies.append(copy)
    for step in master_steps[turns[0] : turns[1]]:
        step()
    for copy in square_copies:
        copy.wait_recv()
    chip_square[...] = jnp.sum(squares[...], axis=0)
    chip_squares[0] = jnp.sum(squares[...], axis=0)
    chip_copies = []
    for k in range(1, tp):
        copy = pltpu.make_async_remote_copy(
            src_ref=chip_square,
            dst_ref=chip_squares.at[k],
            send_sem=chip_send.at[k],
            recv_sem=chip_recv.at[k],
            device_id={"tp": lax.rem(my_tp + k, tp)},
            device_id_type=MESH,
        )
        copy.start()
        chip_copies.append(copy)
    for copy in chip_copies:
        copy.wait_recv()
    total = jnp.sum(chip_squares[...], axis=0)[0:1, 0:1]
    grad_scale = 1.0 / jnp.sqrt(total / count + norm_eps)

    def update(scaled, first, second, base):
        moved = beta_first * first[...] + (1.0 - beta_first) * scaled
        spread = beta_second * second[...] + (1.0 - beta_second) * scaled * scaled
        turned = (moved / (jnp.sqrt(spread) + epsilon)).astype(BF16)
        direction[:, base : base + turned.shape[1]] = turned
        dirs_all[me, :, base : base + turned.shape[1]] = turned

    for load in loads[6:]:
        load.wait()
    scaled = low * grad_scale
    scaled_out[...] = scaled
    update(scaled[:, :kc], first_key, second_key, 0)
    update(scaled[:, kc:], first_value, second_value, kc)

    dirs_g.along_z()
    dirs_steps, dirs_tail = dirs_g.steps()
    dirs_steps[0]()
    for step in master_steps[turns[1] : turns[2]] + dirs_steps[1:] + master_steps[turns[2] :]:
        step()
    for step in dirs_tail + master_tail:
        step()
    for g in (basis_g, master_g, dirs_g):
        g.close()
    for copy in part_copies + square_copies + chip_copies:
        copy.wait_send()


def final_kernel(
    basis_all,
    master_all,
    dirs,
    basis,
    master_key,
    master_value,
    scaled,
    first_key,
    second_key,
    first_value,
    second_value,
    copy_key,
    copy_value,
    step_key,
    step_value,
    new_key,
    new_value,
    new_first_key,
    new_second_key,
    new_first_value,
    new_second_value,
):
    kc = copy_key.shape[1]
    for cut, out in ((slice(0, kc), copy_key), (slice(kc, None), copy_value)):
        step = jnp.dot(basis_all[...], dirs[:, cut], preferred_element_type=F32)
        out[...] = (master_all[:, cut].astype(F32) - learn_rate * step).astype(BF16)

    @pl.when(pl.program_id(0) == 0)
    def _():
        for cut, master, step_out, new in (
            (slice(0, kc), master_key, step_key, new_key),
            (slice(kc, None), master_value, step_value, new_value),
        ):
            step = jnp.dot(basis[...], dirs[:, cut], preferred_element_type=F32)
            step_out[...] = step
            new[...] = master[...] - learn_rate * step
        for cut, first, second, new_first, new_second in (
            (slice(0, kc), first_key, second_key, new_first_key, new_second_key),
            (slice(kc, None), first_value, second_value, new_first_value, new_second_value),
        ):
            own = scaled[:, cut]
            new_first[...] = beta_first * first[...] + (1.0 - beta_first) * own
            new_second[...] = beta_second * second[...] + (1.0 - beta_second) * own * own


def on_device(
    n,
    tp,
    normed,
    key_cot,
    value_cot,
    basis,
    master_key,
    master_value,
    first_key,
    second_key,
    first_value,
    second_value,
):
    rows, rank = basis.shape
    d = rows * n
    kc, vc = key_cot.shape[1], value_cot.shape[1]
    cols = kc + vc
    tokens = normed.shape[0]
    rank_rows = first_key.shape[0]
    lines = n // 4
    vmem = pl.BlockSpec(memory_space=pltpu.VMEM)
    hbm = pl.BlockSpec(memory_space=pl.ANY)
    dma = pltpu.SemaphoreType.DMA
    small = (8, 128)
    basis_all, master_all, dirs, scaled = pl.pallas_call(
        functools.partial(exchange_kernel, n, tp, rank * cols * tp),
        out_shape=(
            jax.ShapeDtypeStruct((d, rank), BF16),
            jax.ShapeDtypeStruct((d, cols), BF16),
            jax.ShapeDtypeStruct((n, rank_rows, cols), BF16),
            jax.ShapeDtypeStruct((rank_rows, cols), F32),
        ),
        in_specs=[hbm] * 10,
        out_specs=[vmem] * 4,
        scratch_shapes=[
            pltpu.VMEM(normed.shape, BF16),
            pltpu.VMEM(key_cot.shape, BF16),
            pltpu.VMEM(value_cot.shape, BF16),
            pltpu.VMEM(basis.shape, BF16),
            pltpu.VMEM(master_key.shape, F32),
            pltpu.VMEM(master_value.shape, F32),
            pltpu.VMEM(first_key.shape, F32),
            pltpu.VMEM(first_key.shape, F32),
            pltpu.VMEM(first_value.shape, F32),
            pltpu.VMEM(first_value.shape, F32),
            pltpu.VMEM((rows, cols), BF16),
            pltpu.VMEM((tokens, rank), BF16),
            pltpu.VMEM((n, rank_rows, cols), BF16),
            pltpu.VMEM((n, rank_rows, cols), BF16),
            pltpu.VMEM((rank_rows, cols), BF16),
            pltpu.VMEM(small, F32),
            pltpu.VMEM((n, *small), F32),
            pltpu.VMEM(small, F32),
            pltpu.VMEM((tp, *small), F32),
            dma((10,)),
        ]
        + [dma((2, 4 * lines))] * 6
        + [dma((n,))] * 4
        + [dma((tp,))] * 2,
        compiler_params=pltpu.CompilerParams(
            collective_id=0, has_side_effects=True, vmem_limit_bytes=67_043_328
        ),
    )(normed, key_cot, value_cot, basis, master_key, master_value, first_key, second_key, first_value, second_value)
    dirs = dirs.reshape(rank, cols)

    block = d // 2
    whole = lambda *shape: pl.BlockSpec(shape, lambda i: (0,) * len(shape))
    sliced = lambda width: pl.BlockSpec((block, width), lambda i: (i, 0))
    moments = [whole(rank_rows, kc)] * 2 + [whole(rank_rows, vc)] * 2
    copy_key, copy_value, step_key, step_value, new_key, new_value, nfk, nsk, nfv, nsv = pl.pallas_call(
        final_kernel,
        grid=(d // block,),
        out_shape=(
            jax.ShapeDtypeStruct((d, kc), BF16),
            jax.ShapeDtypeStruct((d, vc), BF16),
            jax.ShapeDtypeStruct((rows, kc), F32),
            jax.ShapeDtypeStruct((rows, vc), F32),
            jax.ShapeDtypeStruct((rows, kc), F32),
            jax.ShapeDtypeStruct((rows, vc), F32),
            jax.ShapeDtypeStruct(first_key.shape, F32),
            jax.ShapeDtypeStruct(first_key.shape, F32),
            jax.ShapeDtypeStruct(first_value.shape, F32),
            jax.ShapeDtypeStruct(first_value.shape, F32),
        ),
        in_specs=[
            sliced(rank),
            sliced(cols),
            whole(rank, cols),
            whole(rows, rank),
            whole(rows, kc),
            whole(rows, vc),
            whole(rank_rows, cols),
            *moments,
        ],
        out_specs=[sliced(kc), sliced(vc), whole(rows, kc), whole(rows, vc), whole(rows, kc), whole(rows, vc), *moments],
    )(
        basis_all, master_all, dirs, basis, master_key, master_value, scaled, first_key, second_key, first_value, second_value
    )
    return (step_key, step_value, new_key, new_value, copy_key, copy_value, nfk, nsk, nfv, nsv)


def solution(mesh):
    split = P("fs", "tp")
    lone = P("fs", None)
    return jax.shard_map(
        functools.partial(on_device, mesh.shape["fs"], mesh.shape["tp"]),
        mesh=mesh,
        in_specs=(lone, split, split, lone) + (split,) * 6,
        out_specs=(split,) * 4 + (P(None, "tp"),) * 2 + (split,) * 4,
        check_vma=False,
    )
```

profile of v0, /device:TPU:8, one launch (start us, length us, event | category | flops | bytes accessed | tf_op | source)
XLA Modules:
  0.0 158.1 jit_solution(16615404356389299379)
XLA Ops:
  0.6 152.3 %shard_map.177 = (bf16[2048,256]{1,0:T(8,128)(2,1)}, bf16[2048,384]{1,0:T(8,128)(2,1)}, bf16[64,4,384]{2,1,0:T(4,128)(2,1)}, f32[4,384]{1,0:T(4,128)}) custom-call(bf16[1024,2048]{1,0:T(8,128)(2,1)} %normed.1, bf16[1024,128]{1,0:T(8,128)(2,1)} %key_cot.1, bf16[1024,256]{1,0:T(8,128)(2,1)} %value_cot.1, bf16[32,256]{1,0:T(8,128)(2,1)} %basis.1, ...), custom_call_target="tpu_custom_call" | custom-call | tf_op jit(solution)/shard_map/pallas_call | solution.py:438
  153.0 1.6 %reshape.23.dirs = bf16[256,384]{1,0:T(8,128)(2,1)} reshape(bf16[64,4,384]{2,1,0:T(4,128)(2,1)} %get-tuple-element.26) | data formatting | bytes 393216 | tf_op jit(solution)/shard_map/reshape | solution.py:477
  154.6 3.5 %shard_map.178 = (bf16[2048,128]{1,0:T(8,128)(2,1)}, bf16[2048,256]{1,0:T(8,128)(2,1)}, f32[32,128]{1,0:T(8,128)}, f32[32,256]{1,0:T(8,128)}, f32[32,128]{1,0:T(...) custom-call(bf16[2048,256]{1,0:T(8,128)(2,1)} %get-tuple-element.24., ...), custom_call_target="tpu_custom_call" | custom-call | tf_op jit(solution)/shard_map/pallas_call | solution.py:483
where the time goes:
time: 158 us
  Pallas kernels  156 us (99%)
  local copies, waits for them, and re-layouts  1.65 us (1%)
    pallas_call x1, Pallas kernels, on_device(): pl.pallas_call(functools.partial(exchange_kernel, n, tp, rank * cols * tp...  152 us
    pallas_call x1, Pallas kernels, on_device(): pl.pallas_call(final_kernel, grid=(d // block,), out_shape=(jax.ShapeDtyp...  3.45 us

commit v1 on v0

v1 whole, which is shorter than its diff:
```python
import functools

import jax
import jax.numpy as jnp
from jax import lax
from jax.experimental import pallas as pl
from jax.experimental.pallas import tpu as pltpu
from jax.sharding import PartitionSpec as P

learn_rate = 0.05
beta_first = 0.9
beta_second = 0.9
epsilon = 1e-08
norm_eps = 1e-06

MESH = pl.DeviceIdType.MESH
F32 = jnp.float32
BF16 = jnp.bfloat16
SIDE = 8
NEAR = (1, 7, 2, 6, 3, 5, 4)
FAR = (4, 3, 5, 2, 6, 1, 7)


def distance(k):
    return min(k, SIDE - k)


def wait_recv(ref, sem):
    pltpu.make_async_remote_copy(
        src_ref=ref, dst_ref=ref, send_sem=sem, recv_sem=sem, device_id={"fs": 0}, device_id_type=MESH
    ).wait_recv()


def wait_send(ref, sem):
    pltpu.make_async_remote_copy(
        src_ref=ref, dst_ref=ref, send_sem=sem, recv_sem=sem, device_id={"fs": 0}, device_id_type=MESH
    ).wait_send()


def send(ref, target_ref, send_sem, recv_sem, **device):
    pltpu.make_async_remote_copy(
        src_ref=ref,
        dst_ref=target_ref,
        send_sem=send_sem,
        recv_sem=recv_sem,
        device_id=device,
        device_id_type=MESH,
    ).start()


def exchange_kernel(
    n,
    tp,
    count,
    normed,
    key_cot,
    value_cot,
    basis_in,
    master_key,
    master_value,
    first_key_in,
    second_key_in,
    first_value_in,
    second_value_in,
    basis_all,
    master_all,
    dirs,
    scaled_out,
    normed_v,
    key_v,
    value_v,
    master_key_v,
    master_value_v,
    first_key,
    second_key,
    first_value,
    second_value,
    moments,
    cot_t,
    grad_t,
    partial,
    received,
    low_own,
    low_all,
    turned,
    chip_own,
    chip_all,
    square_own,
    square_all,
    load_sem,
    basis_send,
    basis_one,
    basis_two,
    core_send,
    core_one,
    core_two,
    pack_send,
    pack_one,
    pack_near,
    part_send,
    part_recv,
    low_send,
    low_recv,
    chip_send,
    chip_recv,
    square_send,
    square_recv,
):
    me = lax.axis_index("fs")
    my_tp = lax.axis_index("tp")
    z, y = me // SIDE, lax.rem(me, SIDE)
    core = lax.rem(my_tp, 2)
    partner = my_tp + 1 - 2 * core

    def along(part, k):
        if part == 0:
            return lax.rem(z + k, SIDE) * SIDE + y
        return z * SIDE + lax.rem(y + k, SIDE)

    rows = basis_in.shape[0]
    half = rows // 2
    kc = key_cot.shape[1]

    loads = [
        pltpu.make_async_copy(source, target, load_sem.at[i])
        for i, (source, target) in enumerate(
            (
                (basis_in.at[:, 0:128], basis_all.at[0, z, y]),
                (basis_in.at[:, 128:256], basis_all.at[1, z, y]),
                (master_key, master_key_v),
                (master_value, master_value_v),
                (first_key_in, first_key),
                (second_key_in, second_key),
                (first_value_in, first_value),
                (second_value_in, second_value),
                (key_cot, key_v),
                (value_cot, value_v),
                (normed, normed_v),
            )
        )
    ]
    for load in loads:
        load.start()

    barrier = pltpu.get_barrier_semaphore()
    for k in range(1, SIDE):
        pl.semaphore_signal(barrier, inc=1, device_id={"fs": along(0, k)}, device_id_type=MESH)
        pl.semaphore_signal(barrier, inc=1, device_id={"fs": along(1, k)}, device_id_type=MESH)
    for k in range(1, tp):
        pl.semaphore_signal(barrier, inc=1, device_id={"tp": lax.rem(my_tp + k, tp)}, device_id_type=MESH)

    for load in loads[2:8]:
        load.wait()
    master_all[z, y, :, :kc] = master_key_v[...].astype(BF16)
    master_all[z, y, :, kc:] = master_value_v[...].astype(BF16)
    moments[0, z, y, :, :kc] = first_key[...].astype(BF16)
    moments[0, z, y, :, kc:] = first_value[...].astype(BF16)
    moments[1, z, y, :, :kc] = second_key[...].astype(BF16)
    moments[1, z, y, :, kc:] = second_value[...].astype(BF16)
    loads[0].wait()
    loads[1].wait()

    pl.semaphore_wait(barrier, 2 * (SIDE - 1) + tp - 1)

    spans = (pl.ds(0, half), pl.ds(half, half))

    def basis_at(part, zz, yy):
        return basis_all.at[core, zz, yy, spans[part], :]

    def basis_group(part, k):
        if part == 0:
            return basis_all.at[core, :, lax.rem(y + k, SIDE), spans[0], :]
        return basis_all.at[core, lax.rem(z + k, SIDE), :, spans[1], :]

    def other_group(part, k):
        if part == 0:
            return basis_all.at[1 - core, :, lax.rem(y + k, SIDE), spans[0], :]
        return basis_all.at[1 - core, lax.rem(z + k, SIDE), :, spans[1], :]

    def line_at(part, k):
        if part == 0:
            return lax.rem(z + k, SIDE), y
        return z, lax.rem(y + k, SIDE)

    for k in FAR:
        for part in range(2):
            own = basis_at(part, z, y)
            send(own, own, basis_send.at[part], basis_one.at[part, k], fs=along(part, k))

    for j in (0,) + NEAR:
        for part in range(2):
            block = basis_at(part, *line_at(part, SIDE - j))
            if j:
                wait_recv(block, basis_one.at[part, j])
            for k in FAR:
                send(block, block, basis_send.at[2 + part], basis_two.at[part, k], fs=along(1 - part, k))
            if j:
                send(block, block, core_send.at[part], core_one.at[part, j], tp=partner)

    def pack_at(part, zz, yy):
        return master_all.at[zz, yy, spans[part], :], moments.at[part, zz, yy]

    def pack_group(part, k, cut=slice(None)):
        cut = pl.ds(cut.start, cut.stop - cut.start) if cut.start is not None else slice(None)
        if part == 0:
            at = lax.rem(y + k, SIDE)
            return master_all.at[cut, at, spans[0], :], moments.at[0, cut, at]
        at = lax.rem(z + k, SIDE)
        return master_all.at[at, cut, spans[1], :], moments.at[1, at, cut]

    for k in FAR:
        for part in range(2):
            for a, block in enumerate(pack_at(part, z, y)):
                send(block, block, pack_send.at[part, a], pack_one.at[part, a, k], fs=along(part, k))

    loads[8].wait()
    loads[9].wait()
    cot_t[:kc, :] = key_v[...].T
    cot_t[kc:, :] = value_v[...].T
    loads[10].wait()
    tile = 256

    @pl.loop(0, normed_v.shape[1] // tile)
    def _(t):
        at = pl.ds(pl.multiple_of(t * tile, tile), tile)
        grad_t[:, at] = jnp.dot(cot_t[...], normed_v[:, at], preferred_element_type=F32).astype(BF16)

    for k in NEAR:
        for part in range(2):
            group = basis_group(part, SIDE - k)
            wait_recv(group, basis_two.at[part, k])
            send(group, group, core_send.at[2 + part], core_two.at[part, k], tp=partner)
    for k in NEAR:
        for part in range(2):
            zz, yy = line_at(part, SIDE - k)
            wait_recv(basis_all.at[1 - core, zz, yy, spans[part], :], core_one.at[part, k])
            wait_recv(other_group(part, SIDE - k), core_two.at[part, k])

    depth = n * rows
    whole = jnp.concatenate(
        [basis_all[0].reshape(depth, 128), basis_all[1].reshape(depth, 128)], axis=1
    )
    sums = jnp.dot(grad_t[...], whole, preferred_element_type=F32).T.astype(BF16)
    rank_rows = first_key.shape[0]
    for j in range(n):
        partial[j] = sums[j * rank_rows : (j + 1) * rank_rows, :]

    order = sorted(
        ((dz, dy) for dz in range(SIDE) for dy in range(SIDE) if dz or dy),
        key=lambda d: -distance(d[0]) - distance(d[1]),
    )

    def device(dz, dy):
        return lax.rem(z + dz, SIDE) * SIDE + lax.rem(y + dy, SIDE)

    for dz, dy in order:
        target = device(dz, dy)
        send(partial.at[target], received.at[dz * SIDE + dy], part_send.at[0], part_recv.at[0], fs=target)

    for k in NEAR:
        for part in range(2):
            for a, block in enumerate(pack_at(part, *line_at(part, SIDE - k))):
                wait_recv(block, pack_one.at[part, a, k])
    for k in (2, 6, 1, 7):
        for part in range(2):
            for a, group in enumerate(pack_group(part, 0)):
                send(group, group, pack_send.at[2 + part, a], pack_near.at[part, a, k], fs=along(1 - part, k))

    wait_recv(received.at[pl.ds(1, n - 1)], part_recv.at[0])
    low = partial[me].astype(F32)
    for k in range(1, n):
        low = low + received[k].astype(F32)

    chip_own[...] = jnp.full(chip_own.shape, jnp.sum(low * low), F32)
    low_own[...] = low.astype(BF16)
    low_all[me] = low.astype(BF16)
    for k in range(1, tp):
        send(chip_own, chip_all.at[k], chip_send.at[0], chip_recv.at[0], tp=lax.rem(my_tp + k, tp))
    for dz, dy in order:
        send(low_own, low_all.at[me], low_send.at[0], low_recv.at[0], fs=device(dz, dy))
    wait_recv(chip_all.at[pl.ds(1, tp - 1)], chip_recv.at[0])
    square = chip_own[...] + jnp.sum(chip_all[1:], axis=0)
    square_own[...] = square
    for dz, dy in order:
        send(square_own, square_all.at[dz * SIDE + dy], square_send.at[0], square_recv.at[0], fs=device(dz, dy))

    for k, ahead, cut in ((2, 1, slice(0, SIDE // 2)), (6, 7, slice(SIDE // 2, SIDE))):
        for part in range(2):
            for a, group in enumerate(pack_group(part, SIDE - k)):
                wait_recv(group, pack_near.at[part, a, k])
                send(
                    group,
                    group,
                    pack_send.at[4 + part, a],
                    pack_near.at[part, a, (k + ahead) % SIDE],
                    fs=along(1 - part, ahead),
                )
            for a, group in enumerate(pack_group(part, SIDE - k, cut)):
                send(
                    group, group, pack_send.at[6 + part, a], pack_near.at[part, a, 0 if k == 2 else 4], fs=along(1 - part, k)
                )

    wait_recv(square_all.at[pl.ds(1, n - 1)], square_recv.at[0])
    total = square_own[...] + jnp.sum(square_all[1:], axis=0)
    grad_scale = (1.0 / jnp.sqrt(total / count + norm_eps))[0:1, 0:1]
    scaled_out[...] = low * grad_scale

    for k in (1, 7, 3, 5):
        for part in range(2):
            for a, group in enumerate(pack_group(part, SIDE - k)):
                wait_recv(group, pack_near.at[part, a, k])
    for slot, cut in ((0, slice(0, SIDE // 2)), (4, slice(SIDE // 2, SIDE))):
        for part in range(2):
            for a, group in enumerate(pack_group(part, SIDE // 2, cut)):
                wait_recv(group, pack_near.at[part, a, slot])
    wait_recv(low_all.at[pl.ds(0, n - 1)], low_recv.at[0])

    for j in range(n):
        scaled = low_all[j].astype(F32) * grad_scale
        moved = beta_first * moments[0, j // SIDE, j % SIDE].astype(F32) + (1.0 - beta_first) * scaled
        spread = beta_second * moments[1, j // SIDE, j % SIDE].astype(F32) + (1.0 - beta_second) * scaled * scaled
        turned[j * rank_rows : (j + 1) * rank_rows, :] = moved / (jnp.sqrt(spread) + epsilon)
    dirs[...] = turned[...].astype(BF16)

    own_line = basis_all.at[0, pl.ds(0, SIDE - 1), 0, spans[0], :]
    for part in range(2):
        wait_send(own_line, basis_send.at[part])
        wait_send(own_line, core_send.at[part])
        wait_send(basis_all.at[0, :, pl.ds(0, SIDE - 1), spans[0], :], basis_send.at[2 + part])
        wait_send(basis_all.at[0, :, pl.ds(0, SIDE - 1), spans[0], :], core_send.at[2 + part])
        for a, array in enumerate((lambda *at: master_all.at[(*at, spans[0])], lambda *at: moments.at[(0, *at)])):
            wait_send(array(pl.ds(0, SIDE - 1), 0), pack_send.at[part, a])
            wait_send(array(slice(None), pl.ds(0, 4)), pack_send.at[2 + part, a])
            wait_send(array(slice(None), pl.ds(0, 2)), pack_send.at[4 + part, a])
            wait_send(array(slice(None), 0), pack_send.at[6 + part, a])
    wait_send(partial.at[pl.ds(0, n - 1)], part_send.at[0])
    wait_send(low_all.at[pl.ds(0, n - 1)], low_send.at[0])
    wait_send(chip_all.at[pl.ds(1, tp - 1)], chip_send.at[0])
    wait_send(square_all.at[pl.ds(1, n - 1)], square_send.at[0])


def final_kernel(
    basis_all,
    master_all,
    dirs,
    basis,
    master_key,
    master_value,
    scaled,
    first_key,
    second_key,
    first_value,
    second_value,
    copy_key,
    copy_value,
    step_key,
    step_value,
    new_key,
    new_value,
    new_first_key,
    new_second_key,
    new_first_value,
    new_second_value,
):
    kc = copy_key.shape[1]
    whole = jnp.concatenate([basis_all[0], basis_all[1]], axis=1)
    for cut, out in ((slice(0, kc), copy_key), (slice(kc, None), copy_value)):
        step = jnp.dot(whole, dirs[:, cut], preferred_element_type=F32)
        out[...] = (master_all[:, cut].astype(F32) - learn_rate * step).astype(BF16)

    @pl.when(pl.program_id(0) == 0)
    def _():
        for cut, master, step_out, new in (
            (slice(0, kc), master_key, step_key, new_key),
            (slice(kc, None), master_value, step_value, new_value),
        ):
            step = jnp.dot(basis[...], dirs[:, cut], preferred_element_type=F32)
            step_out[...] = step
            new[...] = master[...] - learn_rate * step
        for cut, first, second, new_first, new_second in (
            (slice(0, kc), first_key, second_key, new_first_key, new_second_key),
            (slice(kc, None), first_value, second_value, new_first_value, new_second_value),
        ):
            own = scaled[:, cut]
            new_first[...] = beta_first * first[...] + (1.0 - beta_first) * own
            new_second[...] = beta_second * second[...] + (1.0 - beta_second) * own * own


def on_device(
    n,
    tp,
    normed,
    key_cot,
    value_cot,
    basis,
    master_key,
    master_value,
    first_key,
    second_key,
    first_value,
    second_value,
):
    rows, rank = basis.shape
    d = rows * n
    kc, vc = key_cot.shape[1], value_cot.shape[1]
    cols = kc + vc
    tokens = normed.shape[0]
    rank_rows = first_key.shape[0]
    vmem = pl.BlockSpec(memory_space=pltpu.VMEM)
    hbm = pl.BlockSpec(memory_space=pl.ANY)
    dma = pltpu.SemaphoreType.DMA
    small = (1, 128)
    basis_all, master_all, dirs, scaled = pl.pallas_call(
        functools.partial(exchange_kernel, n, tp, rank * cols * tp),
        out_shape=(
            jax.ShapeDtypeStruct((2, SIDE, SIDE, rows, rank // 2), BF16),
            jax.ShapeDtypeStruct((SIDE, SIDE, rows, cols), BF16),
            jax.ShapeDtypeStruct((rank, cols), BF16),
            jax.ShapeDtypeStruct((rank_rows, cols), F32),
        ),
        in_specs=[hbm] * 10,
        out_specs=[vmem] * 4,
        scratch_shapes=[
            pltpu.VMEM(normed.shape, BF16),
            pltpu.VMEM(key_cot.shape, BF16),
            pltpu.VMEM(value_cot.shape, BF16),
            pltpu.VMEM(master_key.shape, F32),
            pltpu.VMEM(master_value.shape, F32),
            pltpu.VMEM(first_key.shape, F32),
            pltpu.VMEM(first_key.shape, F32),
            pltpu.VMEM(first_value.shape, F32),
            pltpu.VMEM(first_value.shape, F32),
            pltpu.VMEM((2, SIDE, SIDE, rank_rows, cols), BF16),
            pltpu.VMEM((cols, tokens), BF16),
            pltpu.VMEM((cols, d), BF16),
            pltpu.VMEM((n, rank_rows, cols), BF16),
            pltpu.VMEM((n, rank_rows, cols), BF16),
            pltpu.VMEM((rank_rows, cols), BF16),
            pltpu.VMEM((n, rank_rows, cols), BF16),
            pltpu.VMEM((rank, cols), F32),
            pltpu.VMEM(small, F32),
            pltpu.VMEM((tp, *small), F32),
            pltpu.VMEM(small, F32),
            pltpu.VMEM((n, *small), F32),
            dma((11,)),
            dma((4,)),
            dma((2, SIDE)),
            dma((2, SIDE)),
            dma((4,)),
            dma((2, SIDE)),
            dma((2, SIDE)),
            dma((8, 2)),
            dma((2, 2, SIDE)),
            dma((2, 2, SIDE)),
        ]
        + [dma((1,))] * 8,
        compiler_params=pltpu.CompilerParams(
            collective_id=0, has_side_effects=True, vmem_limit_bytes=67_043_328
        ),
    )(normed, key_cot, value_cot, basis, master_key, master_value, first_key, second_key, first_value, second_value)
    basis_all = basis_all.reshape(2, d, rank // 2)
    master_all = master_all.reshape(d, cols)

    block = d // 2
    whole = lambda *shape: pl.BlockSpec(shape, lambda i: (0,) * len(shape))
    sliced = lambda width: pl.BlockSpec((block, width), lambda i: (i, 0))
    moments = [whole(rank_rows, kc)] * 2 + [whole(rank_rows, vc)] * 2
    copy_key, copy_value, step_key, step_value, new_key, new_value, nfk, nsk, nfv, nsv = pl.pallas_call(
        final_kernel,
        grid=(d // block,),
        out_shape=(
            jax.ShapeDtypeStruct((d, kc), BF16),
            jax.ShapeDtypeStruct((d, vc), BF16),
            jax.ShapeDtypeStruct((rows, kc), F32),
            jax.ShapeDtypeStruct((rows, vc), F32),
            jax.ShapeDtypeStruct((rows, kc), F32),
            jax.ShapeDtypeStruct((rows, vc), F32),
            jax.ShapeDtypeStruct(first_key.shape, F32),
            jax.ShapeDtypeStruct(first_key.shape, F32),
            jax.ShapeDtypeStruct(first_value.shape, F32),
            jax.ShapeDtypeStruct(first_value.shape, F32),
        ),
        in_specs=[
            pl.BlockSpec((2, block, rank // 2), lambda i: (0, i, 0)),
            sliced(cols),
            whole(rank, cols),
            whole(rows, rank),
            whole(rows, kc),
            whole(rows, vc),
            whole(rank_rows, cols),
            *moments,
        ],
        out_specs=[sliced(kc), sliced(vc), whole(rows, kc), whole(rows, vc), whole(rows, kc), whole(rows, vc), *moments],
    )(
        basis_all, master_all, dirs, basis, master_key, master_value, scaled, first_key, second_key, first_value, second_value
    )
    return (step_key, step_value, new_key, new_value, copy_key, copy_value, nfk, nsk, nfv, nsv)


def solution(mesh):
    split = P("fs", "tp")
    lone = P("fs", None)
    return jax.shard_map(
        functools.partial(on_device, mesh.shape["fs"], mesh.shape["tp"]),
        mesh=mesh,
        in_specs=(lone, split, split, lone) + (split,) * 6,
        out_specs=(split,) * 4 + (P(None, "tp"),) * 2 + (split,) * 4,
        check_vma=False,
    )
```

time: 158 us -> 61.4 us (0.39)
  the two profiles are of different devices: /device:TPU:8 before, /device:TPU:1 now
where the time goes in v1:
time: 61.4 us; the launch traced here: 61.2 us
  Pallas kernels  60.6 us (99%)
  between operations  0.65 us (1%)
    pallas_call x1, Pallas kernels, on_device(): pl.pallas_call(functools.partial(exchange_kernel, n, tp, rank * cols * tp...  57.1 us
    pallas_call x1, Pallas kernels, on_device(): pl.pallas_call(final_kernel, grid=(d // block,), out_shape=(jax.ShapeDtyp...  3.5 us

profile of v1, /device:TPU:1, one launch (start us, length us, event | category | flops | bytes accessed | tf_op | source)
XLA Modules:
  0.0 61.2 jit_solution(11854968117664726173)
XLA Ops:
  0.6 57.1 %shard_map.177 = (bf16[2,8,8,32,128]{4,3,2,1,0:T(8,128)(2,1)}, bf16[8,8,32,384]{3,2,1,0:T(8,128)(2,1)}, bf16[256,384]{1,0:T(8,128)(2,1)}, f32[4,384]{1,0:T(4,128)}) custom-call(bf16[1024,2048]{1,0:T(8,128)(2,1)} %normed.1, bf16[1024,128]{1,0:T(8,128)(2,1)} %key_cot.1, bf16[1024,256]{1,0:T(8,128)(2,1)} %value_cot.1, bf16[32,256]{1,0:T(8,128)(2,1)} %basis.1, ...), custom_call_target="tpu_custom_call" | custom-call | tf_op jit(solution)/shard_map/pallas_call | solution.py:413
  57.7 3.5 %shard_map.178 = (bf16[2048,128]{1,0:T(8,128)(2,1)}, bf16[2048,256]{1,0:T(8,128)(2,1)}, f32[32,128]{1,0:T(8,128)}, f32[32,256]{1,0:T(8,128)}, f32[32,128]{1,0:T(...) custom-call(bf16[2,2048,128]{2,1,0:T(8,128)(2,1)} %bitcast.3, ...), custom_call_target="tpu_custom_call" | custom-call | tf_op jit(solution)/shard_map/pallas_call | solution.py:468

commit v2 on v1

--- a/solution.py
+++ b/solution.py
@@ -139,15 +139,65 @@
             )
         )
     ]
-    for load in loads:
-        load.start()
-
     barrier = pltpu.get_barrier_semaphore()
     for k in range(1, SIDE):
         pl.semaphore_signal(barrier, inc=1, device_id={"fs": along(0, k)}, device_id_type=MESH)
         pl.semaphore_signal(barrier, inc=1, device_id={"fs": along(1, k)}, device_id_type=MESH)
     for k in range(1, tp):
         pl.semaphore_signal(barrier, inc=1, device_id={"tp": lax.rem(my_tp + k, tp)}, device_id_type=MESH)
+
+    for load in loads:
+        load.start()
+
+    loads[0].wait()
+    loads[1].wait()
+    pl.semaphore_wait(barrier, 2 * (SIDE - 1) + tp - 1)
+
+    spans = (pl.ds(0, half), pl.ds(half, half))
+
+    def basis_at(part, zz, yy):
+        return basis_all.at[core, zz, yy, spans[part], :]
+
+    def basis_group(part, k):
+        if part == 0:
+            return basis_all.at[core, :, lax.rem(y + k, SIDE), spans[0], :]
+        return basis_all.at[core, lax.rem(z + k, SIDE), :, spans[1], :]
+
+    def other_group(part, k):
+        if part == 0:
+            return basis_all.at[1 - core, :, lax.rem(y + k, SIDE), spans[0], :]
+        return basis_all.at[1 - core, lax.rem(z + k, SIDE), :, spans[1], :]
+
+    def line_at(part, k):
+        if part == 0:
+            return lax.rem(z + k, SIDE), y
+        return z, lax.rem(y + k, SIDE)
+
+    for k in FAR:
+        for part in range(2):
+            own = basis_at(part, z, y)
+            send(own, own, basis_send.at[part], basis_one.at[part, k], fs=along(part, k))
+
+    for j in (0,) + NEAR:
+        for part in range(2):
+            block = basis_at(part, *line_at(part, SIDE - j))
+            if j:
+                wait_recv(block, basis_one.at[part, j])
+            for k in FAR:
+                send(block, block, basis_send.at[2 + part], basis_two.at[part, k], fs=along(1 - part, k))
+            if j:
+                send(block, block, core_send.at[part], core_one.at[part, j], tp=partner)
+
+    def pack_at(part, zz, yy):
+        return master_all.at[zz, yy, spans[part], :], moments.at[part, zz, yy]
+
+    def pack_group(part, k, cut=slice(None)):
+        cut = pl.ds(cut.start, cut.stop - cut.start) if cut.start is not None else slice(None)
+        if part == 0:
+            at = lax.rem(y + k, SIDE)
+            return master_all.at[cut, at, spans[0], :], moments.at[0, cut, at]
+        at = lax.rem(z + k, SIDE)
+        return master_all.at[at, cut, spans[1], :], moments.at[1, at, cut]
 
     for load in loads[2:8]:
         load.wait()
@@ -157,61 +207,45 @@
     moments[0, z, y, :, kc:] = first_value[...].astype(BF16)
     moments[1, z, y, :, :kc] = second_key[...].astype(BF16)
     moments[1, z, y, :, kc:] = second_value[...].astype(BF16)
-    loads[0].wait()
-    loads[1].wait()
-
-    pl.semaphore_wait(barrier, 2 * (SIDE - 1) + tp - 1)
-
-    spans = (pl.ds(0, half), pl.ds(half, half))
-
-    def basis_at(part, zz, yy):
-        return basis_all.at[core, zz, yy, spans[part], :]
-
-    def basis_group(part, k):
-        if part == 0:
-            return basis_all.at[core, :, lax.rem(y + k, SIDE), spans[0], :]
-        return basis_all.at[core, lax.rem(z + k, SIDE), :, spans[1], :]
-
-    def other_group(part, k):
-        if part == 0:
-            return basis_all.at[1 - core, :, lax.rem(y + k, SIDE), spans[0], :]
-        return basis_all.at[1 - core, lax.rem(z + k, SIDE), :, spans[1], :]
-
-    def line_at(part, k):
-        if part == 0:
-            return lax.rem(z + k, SIDE), y
-        return z, lax.rem(y + k, SIDE)
-
-    for k in FAR:
-        for part in range(2):
-            own = basis_at(part, z, y)
-            send(own, own, basis_send.at[part], basis_one.at[part, k], fs=along(part, k))
-
-    for j in (0,) + NEAR:
-        for part in range(2):
-            block = basis_at(part, *line_at(part, SIDE - j))
-            if j:
-                wait_recv(block, basis_one.at[part, j])
-            for k in FAR:
-                send(block, block, basis_send.at[2 + part], basis_two.at[part, k], fs=along(1 - part, k))
-            if j:
-                send(block, block, core_send.at[part], core_one.at[part, j], tp=partner)
-
-    def pack_at(part, zz, yy):
-        return master_all.at[zz, yy, spans[part], :], moments.at[part, zz, yy]
-
-    def pack_group(part, k, cut=slice(None)):
-        cut = pl.ds(cut.start, cut.stop - cut.start) if cut.start is not None else slice(None)
-        if part == 0:
-            at = lax.rem(y + k, SIDE)
-            return master_all.at[cut, at, spans[0], :], moments.at[0, cut, at]
-        at = lax.rem(z + k, SIDE)
-        return master_all.at[at, cut, spans[1], :], moments.at[1, at, cut]
 
     for k in FAR:
         for part in range(2):
             for a, block in enumerate(pack_at(part, z, y)):
                 send(block, block, pack_send.at[part, a], pack_one.at[part, a, k], fs=along(part, k))
+
+    def pack_first():
+        for k in NEAR:
+            for part in range(2):
+                for a, block in enumerate(pack_at(part, *line_at(part, SIDE - k))):
+                    wait_recv(block, pack_one.at[part, a, k])
+        for k in (1, 7):
+            for part in range(2):
+                for a, group in enumerate(pack_group(part, 0)):
+                    send(group, group, pack_send.at[2 + part, a], pack_near.at[part, a, k], fs=along(1 - part, k))
+
+    def pack_step(k):
+        ahead = 1 if k < SIDE // 2 else SIDE - 1
+        for part in range(2):
+            for a, group in enumerate(pack_group(part, SIDE - k)):
+                wait_recv(group, pack_near.at[part, a, k])
+                send(
+                    group,
+                    group,
+                    pack_send.at[4 + part, a],
+                    pack_near.at[part, a, (k + ahead) % SIDE],
+                    fs=along(1 - part, ahead),
+                )
+        if distance(k) == 2:
+            cut = slice(0, SIDE // 2) if k == 2 else slice(SIDE // 2, SIDE)
+            for part in range(2):
+                for a, group in enumerate(pack_group(part, SIDE - k, cut)):
+                    send(
+                        group,
+                        group,
+                        pack_send.at[6 + part, a],
+                        pack_near.at[part, a, 0 if k == 2 else 4],
+                        fs=along(1 - part, k),
+                    )
 
     loads[8].wait()
     loads[9].wait()
@@ -225,6 +259,7 @@
         at = pl.ds(pl.multiple_of(t * tile, tile), tile)
         grad_t[:, at] = jnp.dot(cot_t[...], normed_v[:, at], preferred_element_type=F32).astype(BF16)
 
+    pack_first()
     for k in NEAR:
         for part in range(2):
             group = basis_group(part, SIDE - k)
@@ -257,14 +292,8 @@
         target = device(dz, dy)
         send(partial.at[target], received.at[dz * SIDE + dy], part_send.at[0], part_recv.at[0], fs=target)
 
-    for k in NEAR:
-        for part in range(2):
-            for a, block in enumerate(pack_at(part, *line_at(part, SIDE - k))):
-                wait_recv(block, pack_one.at[part, a, k])
-    for k in (2, 6, 1, 7):
-        for part in range(2):
-            for a, group in enumerate(pack_group(part, 0)):
-                send(group, group, pack_send.at[2 + part, a], pack_near.at[part, a, k], fs=along(1 - part, k))
+    pack_step(1)
+    pack_step(7)
 
     wait_recv(received.at[pl.ds(1, n - 1)], part_recv.at[0])
     low = partial[me].astype(F32)
@@ -284,28 +313,15 @@
     for dz, dy in order:
         send(square_own, square_all.at[dz * SIDE + dy], square_send.at[0], square_recv.at[0], fs=device(dz, dy))
 
-    for k, ahead, cut in ((2, 1, slice(0, SIDE // 2)), (6, 7, slice(SIDE // 2, SIDE))):
-        for part in range(2):
-            for a, group in enumerate(pack_group(part, SIDE - k)):
-                wait_recv(group, pack_near.at[part, a, k])
-                send(
-                    group,
-                    group,
-                    pack_send.at[4 + part, a],
-                    pack_near.at[part, a, (k + ahead) % SIDE],
-                    fs=along(1 - part, ahead),
-                )
-            for a, group in enumerate(pack_group(part, SIDE - k, cut)):
-                send(
-                    group, group, pack_send.at[6 + part, a], pack_near.at[part, a, 0 if k == 2 else 4], fs=along(1 - part, k)
-                )
+    pack_step(2)
+    pack_step(6)
 
     wait_recv(square_all.at[pl.ds(1, n - 1)], square_recv.at[0])
     total = square_own[...] + jnp.sum(square_all[1:], axis=0)
     grad_scale = (1.0 / jnp.sqrt(total / count + norm_eps))[0:1, 0:1]
     scaled_out[...] = low * grad_scale
 
-    for k in (1, 7, 3, 5):
+    for k in (3, 5):
         for part in range(2):
             for a, group in enumerate(pack_group(part, SIDE - k)):
                 wait_recv(group, pack_near.at[part, a, k])
@@ -330,8 +346,8 @@
         wait_send(basis_all.at[0, :, pl.ds(0, SIDE - 1), spans[0], :], core_send.at[2 + part])
         for a, array in enumerate((lambda *at: master_all.at[(*at, spans[0])], lambda *at: moments.at[(0, *at)])):
             wait_send(array(pl.ds(0, SIDE - 1), 0), pack_send.at[part, a])
-            wait_send(array(slice(None), pl.ds(0, 4)), pack_send.at[2 + part, a])
-            wait_send(array(slice(None), pl.ds(0, 2)), pack_send.at[4 + part, a])
+            wait_send(array(slice(None), pl.ds(0, 2)), pack_send.at[2 + part, a])
+            wait_send(array(slice(None), pl.ds(0, 4)), pack_send.at[4 + part, a])
             wait_send(array(slice(None), 0), pack_send.at[6 + part, a])
     wait_send(partial.at[pl.ds(0, n - 1)], part_send.at[0])
     wait_send(low_all.at[pl.ds(0, n - 1)], low_send.at[0])
@@ -363,27 +379,30 @@
     new_second_value,
 ):
     kc = copy_key.shape[1]
-    whole = jnp.concatenate([basis_all[0], basis_all[1]], axis=1)
-    for cut, out in ((slice(0, kc), copy_key), (slice(kc, None), copy_value)):
-        step = jnp.dot(whole, dirs[:, cut], preferred_element_type=F32)
-        out[...] = (master_all[:, cut].astype(F32) - learn_rate * step).astype(BF16)
-
-    @pl.when(pl.program_id(0) == 0)
-    def _():
-        for cut, master, step_out, new in (
-            (slice(0, kc), master_key, step_key, new_key),
-            (slice(kc, None), master_value, step_value, new_value),
-        ):
-            step = jnp.dot(basis[...], dirs[:, cut], preferred_element_type=F32)
-            step_out[...] = step
-            new[...] = master[...] - learn_rate * step
-        for cut, first, second, new_first, new_second in (
-            (slice(0, kc), first_key, second_key, new_first_key, new_second_key),
-            (slice(kc, None), first_value, second_value, new_first_value, new_second_value),
-        ):
-            own = scaled[:, cut]
-            new_first[...] = beta_first * first[...] + (1.0 - beta_first) * own
-            new_second[...] = beta_second * second[...] + (1.0 - beta_second) * own * own
+    depth = copy_key.shape[0]
+    block = depth // SIDE
+    for i in range(SIDE):
+        at = slice(i * block, (i + 1) * block)
+        whole = jnp.concatenate([basis_all[h, i].reshape(block, 128) for h in range(2)], axis=1)
+        held = master_all[i].reshape(block, dirs.shape[1])
+        for cut, out in ((slice(0, kc), copy_key), (slice(kc, None), copy_value)):
+            step = jnp.dot(whole, dirs[:, cut], preferred_element_type=F32)
+            out[at, :] = (held[:, cut].astype(F32) - learn_rate * step).astype(BF16)
+
+    for cut, master, step_out, new in (
+        (slice(0, kc), master_key, step_key, new_key),
+        (slice(kc, None), master_value, step_value, new_value),
+    ):
+        step = jnp.dot(basis[...], dirs[:, cut], preferred_element_type=F32)
+        step_out[...] = step
+        new[...] = master[...] - learn_rate * step
+    for cut, first, second, new_first, new_second in (
+        (slice(0, kc), first_key, second_key, new_first_key, new_second_key),
+        (slice(kc, None), first_value, second_value, new_first_value, new_second_value),
+    ):
+        own = scaled[:, cut]
+        new_first[...] = beta_first * first[...] + (1.0 - beta_first) * own
+        new_second[...] = beta_second * second[...] + (1.0 - beta_second) * own * own
 
 
 def on_device(
@@ -407,16 +426,16 @@
     tokens = normed.shape[0]
     rank_rows = first_key.shape[0]
     vmem = pl.BlockSpec(memory_space=pltpu.VMEM)
-    hbm = pl.BlockSpec(memory_space=pl.ANY)
+    hbm = pl.BlockSpec(memory_space=pltpu.HBM)
     dma = pltpu.SemaphoreType.DMA
     small = (1, 128)
     basis_all, master_all, dirs, scaled = pl.pallas_call(
         functools.partial(exchange_kernel, n, tp, rank * cols * tp),
         out_shape=(
-            jax.ShapeDtypeStruct((2, SIDE, SIDE, rows, rank // 2), BF16),
-            jax.ShapeDtypeStruct((SIDE, SIDE, rows, cols), BF16),
-            jax.ShapeDtypeStruct((rank, cols), BF16),
-            jax.ShapeDtypeStruct((rank_rows, cols), F32),
+            pltpu.VMEM((2, SIDE, SIDE, rows, rank // 2), BF16),
+            pltpu.VMEM((SIDE, SIDE, rows, cols), BF16),
+            pltpu.VMEM((rank, cols), BF16),
+            pltpu.VMEM((rank_rows, cols), F32),
         ),
         in_specs=[hbm] * 10,
         out_specs=[vmem] * 4,
@@ -455,19 +474,11 @@
         ]
         + [dma((1,))] * 8,
         compiler_params=pltpu.CompilerParams(
-            collective_id=0, has_side_effects=True, vmem_limit_bytes=67_043_328
+            collective_id=0, has_side_effects=True, vmem_limit_bytes=62_914_560
         ),
     )(normed, key_cot, value_cot, basis, master_key, master_value, first_key, second_key, first_value, second_value)
-    basis_all = basis_all.reshape(2, d, rank // 2)
-    master_all = master_all.reshape(d, cols)
-
-    block = d // 2
-    whole = lambda *shape: pl.BlockSpec(shape, lambda i: (0,) * len(shape))
-    sliced = lambda width: pl.BlockSpec((block, width), lambda i: (i, 0))
-    moments = [whole(rank_rows, kc)] * 2 + [whole(rank_rows, vc)] * 2
     copy_key, copy_value, step_key, step_value, new_key, new_value, nfk, nsk, nfv, nsv = pl.pallas_call(
         final_kernel,
-        grid=(d // block,),
         out_shape=(
             jax.ShapeDtypeStruct((d, kc), BF16),
             jax.ShapeDtypeStruct((d, vc), BF16),
@@ -480,17 +491,9 @@
             jax.ShapeDtypeStruct(first_value.shape, F32),
             jax.ShapeDtypeStruct(first_value.shape, F32),
         ),
-        in_specs=[
-            pl.BlockSpec((2, block, rank // 2), lambda i: (0, i, 0)),
-            sliced(cols),
-            whole(rank, cols),
-            whole(rows, rank),
-            whole(rows, kc),
-            whole(rows, vc),
-            whole(rank_rows, cols),
-            *moments,
-        ],
-        out_specs=[sliced(kc), sliced(vc), whole(rows, kc), whole(rows, vc), whole(rows, kc), whole(rows, vc), *moments],
+        in_specs=[vmem] * 11,
+        out_specs=[vmem] * 10,
+        compiler_params=pltpu.CompilerParams(vmem_limit_bytes=24 << 20),
     )(
         basis_all, master_all, dirs, basis, master_key, master_value, scaled, first_key, second_key, first_value, second_value
     )

time: 61.4 us -> 56.9 us (0.927)
  Pallas kernels: 60.6 us -> 56 us
    pallas_call x1, Pallas kernels: 57.1 us -> 54.1 us  [on_device(): pl.pallas_call(functools.partial(exchange_kernel, n, tp, rank * cols * tp...]
    pallas_call x1, Pallas kernels: 3.5 us -> 1.87 us  [on_device(): pl.pallas_call(final_kernel, out_shape=(jax.ShapeDtypeStruct((d, kc), BF1...]
where the time goes in v2:
time: 56.9 us; the launch traced here: 56.8 us
  Pallas kernels  56 us (98%)
  between operations  0.76 us (1%)
    pallas_call x1, Pallas kernels, on_device(): pl.pallas_call(functools.partial(exchange_kernel, n, tp, rank * cols * tp...  54.1 us
    pallas_call x1, Pallas kernels, on_device(): pl.pallas_call(final_kernel, out_shape=(jax.ShapeDtypeStruct((d, kc), BF1...  1.87 us

profile of v2, /device:TPU:1, one launch (start us, length us, event | category | flops | bytes accessed | tf_op | source)
XLA Modules:
  0.0 56.8 jit_solution(11599964570429759505)
XLA Ops:
  0.6 0.0 copy-start.4
  0.7 0.0 copy-start.3
  0.7 0.0 copy-start.6
  0.7 0.0 copy-start.5
  0.7 0.0 copy-start
  0.7 0.0 copy-start.2
  0.7 0.0 copy-start.1
  0.7 54.1 %shard_map.177 = (bf16[2,8,8,32,128]{4,3,2,1,0:T(8,128)(2,1)S(1)}, bf16[8,8,32,384]{3,2,1,0:T(8,128)(2,1)S(1)}, bf16[256,384]{1,0:T(8,128)(2,1)S(1)}, f32[4,384]{1,0:T(4,128)S(1)}) custom-call(bf16[1024,2048]{1,0:T(8,128)(2,1)} %normed.1, bf16[1024,128]{1,0:T(8,128)(2,1)} %key_cot.1, bf16[1024,256]{1,0:T(8,128)(2,1)} %value_cot.1, bf16[32,256]{1,0:T(8,128)(2,1)} %basis.1, ...), custom_call_target="tpu_custom_call" | custom-call | tf_op jit(solution)/shard_map/pallas_call | solution.py:432
  54.8 0.0 copy-done.4
  54.8 0.0 copy-done.3
  54.9 0.0 copy-done.6
  54.9 0.0 copy-done.5
  54.9 0.0 copy-done
  54.9 0.0 copy-done.2
  54.9 0.0 copy-done.1
  54.9 1.9 %shard_map.178 = (bf16[2048,128]{1,0:T(8,128)(2,1)}, bf16[2048,256]{1,0:T(8,128)(2,1)}, f32[32,128]{1,0:T(8,128)}, f32[32,256]{1,0:T(8,128)}, f32[32,128]{1,0:T(...) custom-call(bf16[2,8,8,32,128]{4,3,2,1,0:T(8,128)(2,1)S(1)} %get-tup, ...), custom_call_target="tpu_custom_call" | custom-call | tf_op jit(solution)/shard_map/pallas_call | solution.py:480
Async XLA Ops:
  0.6 54.2 %copy-start.4 = (f32[4,256]{1,0:T(4,128)S(1)}, f32[4,256]{1,0:T(4,128)}, u32[]{:S(2)}) copy-start(f32[4,256]{1,0:T(4,128)} %second_value.1) | copy-start | bytes 12292
  0.7 54.2 %copy-start.3 = (f32[4,256]{1,0:T(4,128)S(1)}, f32[4,256]{1,0:T(4,128)}, u32[]{:S(2)}) copy-start(f32[4,256]{1,0:T(4,128)} %first_value.1) | copy-start | bytes 12292
  0.7 54.2 %copy-start.6 = (f32[4,128]{1,0:T(4,128)S(1)}, f32[4,128]{1,0:T(4,128)}, u32[]{:S(2)}) copy-start(f32[4,128]{1,0:T(4,128)} %second_key.1) | copy-start | bytes 6148
  0.7 54.2 %copy-start.5 = (f32[4,128]{1,0:T(4,128)S(1)}, f32[4,128]{1,0:T(4,128)}, u32[]{:S(2)}) copy-start(f32[4,128]{1,0:T(4,128)} %first_key.1) | copy-start | bytes 6148
  0.7 54.2 %copy-start = (f32[32,256]{1,0:T(8,128)S(1)}, f32[32,256]{1,0:T(8,128)}, u32[]{:S(2)}) copy-start(f32[32,256]{1,0:T(8,128)} %master_value.3) | copy-start | bytes 98308
  0.7 54.2 %copy-start.2 = (f32[32,128]{1,0:T(8,128)S(1)}, f32[32,128]{1,0:T(8,128)}, u32[]{:S(2)}) copy-start(f32[32,128]{1,0:T(8,128)} %master_key.3) | copy-start | bytes 49156
  0.7 54.2 %copy-start.1 = (bf16[32,256]{1,0:T(8,128)(2,1)S(1)}, bf16[32,256]{1,0:T(8,128)(2,1)}, u32[]{:S(2)}) copy-start(bf16[32,256]{1,0:T(8,128)(2,1)} %basis.1) | copy-start | bytes 49156

commit v3 on v2

--- a/solution.py
+++ b/solution.py
@@ -118,7 +118,6 @@
         return z * SIDE + lax.rem(y + k, SIDE)
 
     rows = basis_in.shape[0]
-    half = rows // 2
     kc = key_cot.shape[1]
 
     loads = [
@@ -149,56 +148,6 @@
     for load in loads:
         load.start()
 
-    loads[0].wait()
-    loads[1].wait()
-    pl.semaphore_wait(barrier, 2 * (SIDE - 1) + tp - 1)
-
-    spans = (pl.ds(0, half), pl.ds(half, half))
-
-    def basis_at(part, zz, yy):
-        return basis_all.at[core, zz, yy, spans[part], :]
-
-    def basis_group(part, k):
-        if part == 0:
-            return basis_all.at[core, :, lax.rem(y + k, SIDE), spans[0], :]
-        return basis_all.at[core, lax.rem(z + k, SIDE), :, spans[1], :]
-
-    def other_group(part, k):
-        if part == 0:
-            return basis_all.at[1 - core, :, lax.rem(y + k, SIDE), spans[0], :]
-        return basis_all.at[1 - core, lax.rem(z + k, SIDE), :, spans[1], :]
-
-    def line_at(part, k):
-        if part == 0:
-            return lax.rem(z + k, SIDE), y
-        return z, lax.rem(y + k, SIDE)
-
-    for k in FAR:
-        for part in range(2):
-            own = basis_at(part, z, y)
-            send(own, own, basis_send.at[part], basis_one.at[part, k], fs=along(part, k))
-
-    for j in (0,) + NEAR:
-        for part in range(2):
-            block = basis_at(part, *line_at(part, SIDE - j))
-            if j:
-                wait_recv(block, basis_one.at[part, j])
-            for k in FAR:
-                send(block, block, basis_send.at[2 + part], basis_two.at[part, k], fs=along(1 - part, k))
-            if j:
-                send(block, block, core_send.at[part], core_one.at[part, j], tp=partner)
-
-    def pack_at(part, zz, yy):
-        return master_all.at[zz, yy, spans[part], :], moments.at[part, zz, yy]
-
-    def pack_group(part, k, cut=slice(None)):
-        cut = pl.ds(cut.start, cut.stop - cut.start) if cut.start is not None else slice(None)
-        if part == 0:
-            at = lax.rem(y + k, SIDE)
-            return master_all.at[cut, at, spans[0], :], moments.at[0, cut, at]
-        at = lax.rem(z + k, SIDE)
-        return master_all.at[at, cut, spans[1], :], moments.at[1, at, cut]
-
     for load in loads[2:8]:
         load.wait()
     master_all[z, y, :, :kc] = master_key_v[...].astype(BF16)
@@ -207,45 +156,89 @@
     moments[0, z, y, :, kc:] = first_value[...].astype(BF16)
     moments[1, z, y, :, :kc] = second_key[...].astype(BF16)
     moments[1, z, y, :, kc:] = second_value[...].astype(BF16)
-
-    for k in FAR:
+    loads[0].wait()
+    loads[1].wait()
+
+    pl.semaphore_wait(barrier, 2 * (SIDE - 1) + tp - 1)
+
+    def by_core(body):
         for part in range(2):
-            for a, block in enumerate(pack_at(part, z, y)):
-                send(block, block, pack_send.at[part, a], pack_one.at[part, a, k], fs=along(part, k))
-
-    def pack_first():
+            pl.when(core == part)(functools.partial(body, part))
+
+    def line_at(part, k):
+        if part == 0:
+            return lax.rem(z + k, SIDE), y
+        return z, lax.rem(y + k, SIDE)
+
+    def group_at(part, k, cut=slice(None)):
+        if part == 0:
+            return cut, lax.rem(y + k, SIDE)
+        return lax.rem(z + k, SIDE), cut
+
+    def pack_arrays(at):
+        return (0, moments.at[(slice(None), *at)]), (1, master_all.at[at])
+
+    def basis_first(part):
+        own = basis_all.at[core, z, y]
+        for k in FAR:
+            send(own, own, basis_send.at[0], basis_one.at[k], fs=along(part, k))
+        for k in FAR:
+            for a, block in pack_arrays((z, y)):
+                send(block, block, pack_send.at[0, a], pack_one.at[a, k], fs=along(part, k))
+        for j in (0,) + NEAR:
+            block = basis_all.at[(core, *line_at(part, SIDE - j))]
+            if j:
+                wait_recv(block, basis_one.at[j])
+            for k in FAR:
+                send(block, block, basis_send.at[1], basis_two.at[k], fs=along(1 - part, k))
+            if j:
+                send(block, block, core_send.at[0], core_one.at[j], tp=partner)
+        pack_first(part)
+
+    def basis_second(part):
         for k in NEAR:
-            for part in range(2):
-                for a, block in enumerate(pack_at(part, *line_at(part, SIDE - k))):
-                    wait_recv(block, pack_one.at[part, a, k])
+            group = basis_all.at[(core, *group_at(part, SIDE - k))]
+            wait_recv(group, basis_two.at[k])
+            send(group, group, core_send.at[1], core_two.at[k], tp=partner)
+        for k in NEAR:
+            wait_recv(basis_all.at[(1 - core, *line_at(1 - part, SIDE - k))], core_one.at[k])
+            wait_recv(basis_all.at[(1 - core, *group_at(1 - part, SIDE - k))], core_two.at[k])
+
+    def pack_first(part):
+        for k in NEAR:
+            for a, block in pack_arrays(line_at(part, SIDE - k)):
+                wait_recv(block, pack_one.at[a, k])
         for k in (1, 7):
-            for part in range(2):
-                for a, group in enumerate(pack_group(part, 0)):
-                    send(group, group, pack_send.at[2 + part, a], pack_near.at[part, a, k], fs=along(1 - part, k))
-
-    def pack_step(k):
+            for a, group in pack_arrays(group_at(part, 0)):
+                send(group, group, pack_send.at[1, a], pack_near.at[a, k], fs=along(1 - part, k))
+
+    def pack_step(k, part):
         ahead = 1 if k < SIDE // 2 else SIDE - 1
-        for part in range(2):
-            for a, group in enumerate(pack_group(part, SIDE - k)):
-                wait_recv(group, pack_near.at[part, a, k])
+        for a, group in pack_arrays(group_at(part, SIDE - k)):
+            wait_recv(group, pack_near.at[a, k])
+            send(group, group, pack_send.at[2, a], pack_near.at[a, (k + ahead) % SIDE], fs=along(1 - part, ahead))
+        if distance(k) == 2:
+            cut = pl.ds(0, SIDE // 2) if k == 2 else pl.ds(SIDE // 2, SIDE // 2)
+            for a, group in pack_arrays(group_at(part, SIDE - k, cut)):
                 send(
                     group,
                     group,
-                    pack_send.at[4 + part, a],
-                    pack_near.at[part, a, (k + ahead) % SIDE],
-                    fs=along(1 - part, ahead),
+                    pack_send.at[3, a],
+                    pack_near.at[a, 0 if k == 2 else 4],
+                    fs=along(1 - part, k),
                 )
-        if distance(k) == 2:
-            cut = slice(0, SIDE // 2) if k == 2 else slice(SIDE // 2, SIDE)
-            for part in range(2):
-                for a, group in enumerate(pack_group(part, SIDE - k, cut)):
-                    send(
-                        group,
-                        group,
-                        pack_send.at[6 + part, a],
-                        pack_near.at[part, a, 0 if k == 2 else 4],
-                        fs=along(1 - part, k),
-                    )
+
+    def pack_pair(k, part):
+        pack_step(k, part)
+        pack_step(SIDE - k, part)
+
+    def pack_last(a, part):
+        for k in (3, 5):
+            wait_recv(pack_arrays(group_at(part, SIDE - k))[a][1], pack_near.at[a, k])
+        for slot, cut in ((0, pl.ds(0, SIDE // 2)), (4, pl.ds(SIDE // 2, SIDE // 2))):
+            wait_recv(pack_arrays(group_at(part, SIDE // 2, cut))[a][1], pack_near.at[a, slot])
+
+    by_core(basis_first)
 
     loads[8].wait()
     loads[9].wait()
@@ -259,17 +252,7 @@
         at = pl.ds(pl.multiple_of(t * tile, tile), tile)
         grad_t[:, at] = jnp.dot(cot_t[...], normed_v[:, at], preferred_element_type=F32).astype(BF16)
 
-    pack_first()
-    for k in NEAR:
-        for part in range(2):
-            group = basis_group(part, SIDE - k)
-            wait_recv(group, basis_two.at[part, k])
-            send(group, group, core_send.at[2 + part], core_two.at[part, k], tp=partner)
-    for k in NEAR:
-        for part in range(2):
-            zz, yy = line_at(part, SIDE - k)
-            wait_recv(basis_all.at[1 - core, zz, yy, spans[part], :], core_one.at[part, k])
-            wait_recv(other_group(part, SIDE - k), core_two.at[part, k])
+    by_core(basis_second)
 
     depth = n * rows
     whole = jnp.concatenate(
@@ -292,8 +275,7 @@
         target = device(dz, dy)
         send(partial.at[target], received.at[dz * SIDE + dy], part_send.at[0], part_recv.at[0], fs=target)
 
-    pack_step(1)
-    pack_step(7)
+    by_core(functools.partial(pack_pair, 1))
 
     wait_recv(received.at[pl.ds(1, n - 1)], part_recv.at[0])
     low = partial[me].astype(F32)
@@ -313,22 +295,14 @@
     for dz, dy in order:
         send(square_own, square_all.at[dz * SIDE + dy], square_send.at[0], square_recv.at[0], fs=device(dz, dy))
 
-    pack_step(2)
-    pack_step(6)
+    by_core(functools.partial(pack_pair, 2))
 
     wait_recv(square_all.at[pl.ds(1, n - 1)], square_recv.at[0])
     total = square_own[...] + jnp.sum(square_all[1:], axis=0)
     grad_scale = (1.0 / jnp.sqrt(total / count + norm_eps))[0:1, 0:1]
     scaled_out[...] = low * grad_scale
 
-    for k in (3, 5):
-        for part in range(2):
-            for a, group in enumerate(pack_group(part, SIDE - k)):
-                wait_recv(group, pack_near.at[part, a, k])
-    for slot, cut in ((0, slice(0, SIDE // 2)), (4, slice(SIDE // 2, SIDE))):
-        for part in range(2):
-            for a, group in enumerate(pack_group(part, SIDE // 2, cut)):
-                wait_recv(group, pack_near.at[part, a, slot])
+    by_core(functools.partial(pack_last, 0))
     wait_recv(low_all.at[pl.ds(0, n - 1)], low_recv.at[0])
 
     for j in range(n):
@@ -338,17 +312,16 @@
         turned[j * rank_rows : (j + 1) * rank_rows, :] = moved / (jnp.sqrt(spread) + epsilon)
     dirs[...] = turned[...].astype(BF16)
 
-    own_line = basis_all.at[0, pl.ds(0, SIDE - 1), 0, spans[0], :]
-    for part in range(2):
-        wait_send(own_line, basis_send.at[part])
-        wait_send(own_line, core_send.at[part])
-        wait_send(basis_all.at[0, :, pl.ds(0, SIDE - 1), spans[0], :], basis_send.at[2 + part])
-        wait_send(basis_all.at[0, :, pl.ds(0, SIDE - 1), spans[0], :], core_send.at[2 + part])
-        for a, array in enumerate((lambda *at: master_all.at[(*at, spans[0])], lambda *at: moments.at[(0, *at)])):
-            wait_send(array(pl.ds(0, SIDE - 1), 0), pack_send.at[part, a])
-            wait_send(array(slice(None), pl.ds(0, 2)), pack_send.at[2 + part, a])
-            wait_send(array(slice(None), pl.ds(0, 4)), pack_send.at[4 + part, a])
-            wait_send(array(slice(None), 0), pack_send.at[6 + part, a])
+    by_core(functools.partial(pack_last, 1))
+
+    blocks = pl.ds(0, SIDE - 1)
+    wait_send(basis_all.at[0, blocks, 0], basis_send.at[0])
+    wait_send(basis_all.at[0, blocks, 0], core_send.at[0])
+    wait_send(basis_all.at[0, :, blocks], basis_send.at[1])
+    wait_send(basis_all.at[0, :, blocks], core_send.at[1])
+    for i, at in enumerate(((blocks, 0), (slice(None), pl.ds(0, 2)), (slice(None), pl.ds(0, 4)), (slice(None), 0))):
+        for a, array in pack_arrays(at):
+            wait_send(array, pack_send.at[i, a])
     wait_send(partial.at[pl.ds(0, n - 1)], part_send.at[0])
     wait_send(low_all.at[pl.ds(0, n - 1)], low_send.at[0])
     wait_send(chip_all.at[pl.ds(1, tp - 1)], chip_send.at[0])
@@ -462,15 +435,15 @@
             pltpu.VMEM(small, F32),
             pltpu.VMEM((n, *small), F32),
             dma((11,)),
-            dma((4,)),
+            dma((2,)),
+            dma((SIDE,)),
+            dma((SIDE,)),
+            dma((2,)),
+            dma((SIDE,)),
+            dma((SIDE,)),
+            dma((4, 2)),
             dma((2, SIDE)),
             dma((2, SIDE)),
-            dma((4,)),
-            dma((2, SIDE)),
-            dma((2, SIDE)),
-            dma((8, 2)),
-            dma((2, 2, SIDE)),
-            dma((2, 2, SIDE)),
         ]
         + [dma((1,))] * 8,
         compiler_params=pltpu.CompilerParams(

time: 56.9 us -> 54.7 us (0.961)
  Pallas kernels: 56 us -> 53.7 us
    pallas_call x1, Pallas kernels: 54.1 us -> 51.9 us  [on_device(): pl.pallas_call(functools.partial(exchange_kernel, n, tp, rank * cols * tp...]
where the time goes in v3:
time: 54.7 us; the launch traced here: 54.5 us
  Pallas kernels  53.7 us (98%)
  between operations  0.76 us (1%)
    pallas_call x1, Pallas kernels, on_device(): pl.pallas_call(functools.partial(exchange_kernel, n, tp, rank * cols * tp...  51.9 us
    pallas_call x1, Pallas kernels, on_device(): pl.pallas_call(final_kernel, out_shape=(jax.ShapeDtypeStruct((d, kc), BF1...  1.87 us

profile of v3, /device:TPU:1, one launch (start us, length us, event | category | flops | bytes accessed | tf_op | source)
XLA Modules:
  0.0 54.5 jit_solution(1477527814712864563)
XLA Ops:
  0.6 0.0 copy-start.4
  0.7 0.0 copy-start.3
  0.7 0.0 copy-start.6
  0.7 0.0 copy-start.5
  0.7 0.0 copy-start
  0.7 0.0 copy-start.2
  0.7 0.0 copy-start.1
  0.7 51.9 %shard_map.177 = (bf16[2,8,8,32,128]{4,3,2,1,0:T(8,128)(2,1)S(1)}, bf16[8,8,32,384]{3,2,1,0:T(8,128)(2,1)S(1)}, bf16[256,384]{1,0:T(8,128)(2,1)S(1)}, f32[4,384]{1,0:T(4,128)S(1)}) custom-call(bf16[1024,2048]{1,0:T(8,128)(2,1)} %normed.1, bf16[1024,128]{1,0:T(8,128)(2,1)} %key_cot.1, bf16[1024,256]{1,0:T(8,128)(2,1)} %value_cot.1, bf16[32,256]{1,0:T(8,128)(2,1)} %basis.1, ...), custom_call_target="tpu_custom_call" | custom-call | tf_op jit(solution)/shard_map/pallas_call | solution.py:405
  52.6 0.0 copy-done.4
  52.6 0.0 copy-done.3
  52.6 0.0 copy-done.6
  52.6 0.0 copy-done.5
  52.6 0.0 copy-done
  52.6 0.0 copy-done.2
  52.6 0.0 copy-done.1
  52.6 1.9 %shard_map.178 = (bf16[2048,128]{1,0:T(8,128)(2,1)}, bf16[2048,256]{1,0:T(8,128)(2,1)}, f32[32,128]{1,0:T(8,128)}, f32[32,256]{1,0:T(8,128)}, f32[32,128]{1,0:T(...) custom-call(bf16[2,8,8,32,128]{4,3,2,1,0:T(8,128)(2,1)S(1)} %get-tup, ...), custom_call_target="tpu_custom_call" | custom-call | tf_op jit(solution)/shard_map/pallas_call | solution.py:453
Async XLA Ops:
  0.6 51.9 %copy-start.4 = (f32[4,256]{1,0:T(4,128)S(1)}, f32[4,256]{1,0:T(4,128)}, u32[]{:S(2)}) copy-start(f32[4,256]{1,0:T(4,128)} %second_value.1) | copy-start | bytes 12292
  0.7 51.9 %copy-start.3 = (f32[4,256]{1,0:T(4,128)S(1)}, f32[4,256]{1,0:T(4,128)}, u32[]{:S(2)}) copy-start(f32[4,256]{1,0:T(4,128)} %first_value.1) | copy-start | bytes 12292
  0.7 51.9 %copy-start.6 = (f32[4,128]{1,0:T(4,128)S(1)}, f32[4,128]{1,0:T(4,128)}, u32[]{:S(2)}) copy-start(f32[4,128]{1,0:T(4,128)} %second_key.1) | copy-start | bytes 6148
  0.7 51.9 %copy-start.5 = (f32[4,128]{1,0:T(4,128)S(1)}, f32[4,128]{1,0:T(4,128)}, u32[]{:S(2)}) copy-start(f32[4,128]{1,0:T(4,128)} %first_key.1) | copy-start | bytes 6148
  0.7 51.9 %copy-start = (f32[32,256]{1,0:T(8,128)S(1)}, f32[32,256]{1,0:T(8,128)}, u32[]{:S(2)}) copy-start(f32[32,256]{1,0:T(8,128)} %master_value.3) | copy-start | bytes 98308
  0.7 51.9 %copy-start.2 = (f32[32,128]{1,0:T(8,128)S(1)}, f32[32,128]{1,0:T(8,128)}, u32[]{:S(2)}) copy-start(f32[32,128]{1,0:T(8,128)} %master_key.3) | copy-start | bytes 49156
  0.7 51.9 %copy-start.1 = (bf16[32,256]{1,0:T(8,128)(2,1)S(1)}, bf16[32,256]{1,0:T(8,128)(2,1)}, u32[]{:S(2)}) copy-start(bf16[32,256]{1,0:T(8,128)(2,1)} %basis.1) | copy-start | bytes 49156

commit v4 on v3

--- a/solution.py
+++ b/solution.py
@@ -217,24 +217,19 @@
         for a, group in pack_arrays(group_at(part, SIDE - k)):
             wait_recv(group, pack_near.at[a, k])
             send(group, group, pack_send.at[2, a], pack_near.at[a, (k + ahead) % SIDE], fs=along(1 - part, ahead))
-        if distance(k) == 2:
-            cut = pl.ds(0, SIDE // 2) if k == 2 else pl.ds(SIDE // 2, SIDE // 2)
-            for a, group in pack_arrays(group_at(part, SIDE - k, cut)):
-                send(
-                    group,
-                    group,
-                    pack_send.at[3, a],
-                    pack_near.at[a, 0 if k == 2 else 4],
-                    fs=along(1 - part, k),
-                )
+
+    def pack_far(part):
+        for k, ahead, slot, start in ((3, 1, 0, 0), (5, 7, 4, SIDE // 2)):
+            for a, group in pack_arrays(group_at(part, SIDE - k)):
+                wait_recv(group, pack_near.at[a, k])
+            for a, group in pack_arrays(group_at(part, SIDE - k, pl.ds(start, SIDE // 2))):
+                send(group, group, pack_send.at[3, a], pack_near.at[a, slot], fs=along(1 - part, ahead))
 
     def pack_pair(k, part):
         pack_step(k, part)
         pack_step(SIDE - k, part)
 
     def pack_last(a, part):
-        for k in (3, 5):
-            wait_recv(pack_arrays(group_at(part, SIDE - k))[a][1], pack_near.at[a, k])
         for slot, cut in ((0, pl.ds(0, SIDE // 2)), (4, pl.ds(SIDE // 2, SIDE // 2))):
             wait_recv(pack_arrays(group_at(part, SIDE // 2, cut))[a][1], pack_near.at[a, slot])
 
@@ -284,18 +279,31 @@
 
     chip_own[...] = jnp.full(chip_own.shape, jnp.sum(low * low), F32)
     low_own[...] = low.astype(BF16)
-    low_all[me] = low.astype(BF16)
+    low_all[z, y] = low.astype(BF16)
     for k in range(1, tp):
         send(chip_own, chip_all.at[k], chip_send.at[0], chip_recv.at[0], tp=lax.rem(my_tp + k, tp))
-    for dz, dy in order:
-        send(low_own, low_all.at[me], low_send.at[0], low_recv.at[0], fs=device(dz, dy))
+
+    def low_first(part):
+        for k in FAR:
+            send(low_own, low_all.at[z, y], low_send.at[0], low_recv.at[0], fs=along(part, k))
+
+    def low_second(part):
+        line = low_all.at[pl.ds(0, SIDE - 1), 0]
+        wait_recv(line, low_recv.at[0])
+        group = low_all.at[group_at(part, 0)]
+        for k in FAR:
+            send(group, group, low_send.at[1], low_recv.at[1], fs=along(1 - part, k))
+
+    by_core(low_first)
+    by_core(functools.partial(pack_pair, 2))
     wait_recv(chip_all.at[pl.ds(1, tp - 1)], chip_recv.at[0])
     square = chip_own[...] + jnp.sum(chip_all[1:], axis=0)
     square_own[...] = square
     for dz, dy in order:
         send(square_own, square_all.at[dz * SIDE + dy], square_send.at[0], square_recv.at[0], fs=device(dz, dy))
 
-    by_core(functools.partial(pack_pair, 2))
+    by_core(low_second)
+    by_core(pack_far)
 
     wait_recv(square_all.at[pl.ds(1, n - 1)], square_recv.at[0])
     total = square_own[...] + jnp.sum(square_all[1:], axis=0)
@@ -303,10 +311,10 @@
     scaled_out[...] = low * grad_scale
 
     by_core(functools.partial(pack_last, 0))
-    wait_recv(low_all.at[pl.ds(0, n - 1)], low_recv.at[0])
+    wait_recv(low_all.at[:, pl.ds(0, SIDE - 1)], low_recv.at[1])
 
     for j in range(n):
-        scaled = low_all[j].astype(F32) * grad_scale
+        scaled = low_all[j // SIDE, j % SIDE].astype(F32) * grad_scale
         moved = beta_first * moments[0, j // SIDE, j % SIDE].astype(F32) + (1.0 - beta_first) * scaled
         spread = beta_second * moments[1, j // SIDE, j % SIDE].astype(F32) + (1.0 - beta_second) * scaled * scaled
         turned[j * rank_rows : (j + 1) * rank_rows, :] = moved / (jnp.sqrt(spread) + epsilon)
@@ -323,7 +331,8 @@
         for a, array in pack_arrays(at):
             wait_send(array, pack_send.at[i, a])
     wait_send(partial.at[pl.ds(0, n - 1)], part_send.at[0])
-    wait_send(low_all.at[pl.ds(0, n - 1)], low_send.at[0])
+    wait_send(low_all.at[blocks, 0], low_send.at[0])
+    wait_send(low_all.at[:, blocks], low_send.at[1])
     wait_send(chip_all.at[pl.ds(1, tp - 1)], chip_send.at[0])
     wait_send(square_all.at[pl.ds(1, n - 1)], square_send.at[0])
 
@@ -428,7 +437,7 @@
             pltpu.VMEM((n, rank_rows, cols), BF16),
             pltpu.VMEM((n, rank_rows, cols), BF16),
             pltpu.VMEM((rank_rows, cols), BF16),
-            pltpu.VMEM((n, rank_rows, cols), BF16),
+            pltpu.VMEM((SIDE, SIDE, rank_rows, cols), BF16),
             pltpu.VMEM((rank, cols), F32),
             pltpu.VMEM(small, F32),
             pltpu.VMEM((tp, *small), F32),
@@ -445,7 +454,7 @@
             dma((2, SIDE)),
             dma((2, SIDE)),
         ]
-        + [dma((1,))] * 8,
+        + [dma((2,))] * 8,
         compiler_params=pltpu.CompilerParams(
             collective_id=0, has_side_effects=True, vmem_limit_bytes=62_914_560
         ),

time: 54.7 us -> 51.9 us (0.949)
  Pallas kernels: 53.7 us -> 50.9 us
    pallas_call x1, Pallas kernels: 51.9 us -> 49 us  [on_device(): pl.pallas_call(functools.partial(exchange_kernel, n, tp, rank * cols * tp...]
where the time goes in v4:
time: 51.9 us; the launch traced here: 51.7 us
  Pallas kernels  50.9 us (98%)
  between operations  0.76 us (1%)
    pallas_call x1, Pallas kernels, on_device(): pl.pallas_call(functools.partial(exchange_kernel, n, tp, rank * cols * tp...  49 us
    pallas_call x1, Pallas kernels, on_device(): pl.pallas_call(final_kernel, out_shape=(jax.ShapeDtypeStruct((d, kc), BF1...  1.87 us

profile of v4, /device:TPU:1, one launch (start us, length us, event | category | flops | bytes accessed | tf_op | source)
XLA Modules:
  0.0 51.7 jit_solution(10576093685536817154)
XLA Ops:
  0.6 0.0 copy-start.4
  0.7 0.0 copy-start.3
  0.7 0.0 copy-start.6
  0.7 0.0 copy-start.5
  0.7 0.0 copy-start
  0.7 0.0 copy-start.2
  0.7 0.0 copy-start.1
  0.7 49.0 %shard_map.177 = (bf16[2,8,8,32,128]{4,3,2,1,0:T(8,128)(2,1)S(1)}, bf16[8,8,32,384]{3,2,1,0:T(8,128)(2,1)S(1)}, bf16[256,384]{1,0:T(8,128)(2,1)S(1)}, f32[4,384]{1,0:T(4,128)S(1)}) custom-call(bf16[1024,2048]{1,0:T(8,128)(2,1)} %normed.1, bf16[1024,128]{1,0:T(8,128)(2,1)} %key_cot.1, bf16[1024,256]{1,0:T(8,128)(2,1)} %value_cot.1, bf16[32,256]{1,0:T(8,128)(2,1)} %basis.1, ...), custom_call_target="tpu_custom_call" | custom-call | tf_op jit(solution)/shard_map/pallas_call | solution.py:414
  49.8 0.0 copy-done.4
  49.8 0.0 copy-done.3
  49.8 0.0 copy-done.6
  49.8 0.0 copy-done.5
  49.8 0.0 copy-done
  49.8 0.0 copy-done.2
  49.8 0.0 copy-done.1
  49.8 1.9 %shard_map.178 = (bf16[2048,128]{1,0:T(8,128)(2,1)}, bf16[2048,256]{1,0:T(8,128)(2,1)}, f32[32,128]{1,0:T(8,128)}, f32[32,256]{1,0:T(8,128)}, f32[32,128]{1,0:T(...) custom-call(bf16[2,8,8,32,128]{4,3,2,1,0:T(8,128)(2,1)S(1)} %get-tup, ...), custom_call_target="tpu_custom_call" | custom-call | tf_op jit(solution)/shard_map/pallas_call | solution.py:462
Async XLA Ops:
  0.6 49.1 %copy-start.4 = (f32[4,256]{1,0:T(4,128)S(1)}, f32[4,256]{1,0:T(4,128)}, u32[]{:S(2)}) copy-start(f32[4,256]{1,0:T(4,128)} %second_value.1) | copy-start | bytes 12292
  0.7 49.1 %copy-start.3 = (f32[4,256]{1,0:T(4,128)S(1)}, f32[4,256]{1,0:T(4,128)}, u32[]{:S(2)}) copy-start(f32[4,256]{1,0:T(4,128)} %first_value.1) | copy-start | bytes 12292
  0.7 49.1 %copy-start.6 = (f32[4,128]{1,0:T(4,128)S(1)}, f32[4,128]{1,0:T(4,128)}, u32[]{:S(2)}) copy-start(f32[4,128]{1,0:T(4,128)} %second_key.1) | copy-start | bytes 6148
  0.7 49.1 %copy-start.5 = (f32[4,128]{1,0:T(4,128)S(1)}, f32[4,128]{1,0:T(4,128)}, u32[]{:S(2)}) copy-start(f32[4,128]{1,0:T(4,128)} %first_key.1) | copy-start | bytes 6148
  0.7 49.1 %copy-start = (f32[32,256]{1,0:T(8,128)S(1)}, f32[32,256]{1,0:T(8,128)}, u32[]{:S(2)}) copy-start(f32[32,256]{1,0:T(8,128)} %master_value.3) | copy-start | bytes 98308
  0.7 49.1 %copy-start.2 = (f32[32,128]{1,0:T(8,128)S(1)}, f32[32,128]{1,0:T(8,128)}, u32[]{:S(2)}) copy-start(f32[32,128]{1,0:T(8,128)} %master_key.3) | copy-start | bytes 49156
  0.7 49.1 %copy-start.1 = (bf16[32,256]{1,0:T(8,128)(2,1)S(1)}, bf16[32,256]{1,0:T(8,128)(2,1)}, u32[]{:S(2)}) copy-start(bf16[32,256]{1,0:T(8,128)(2,1)} %basis.1) | copy-start | bytes 49156

commit v5 on v4

--- a/solution.py
+++ b/solution.py
@@ -82,7 +82,10 @@
     received,
     low_own,
     low_all,
-    turned,
+    low_part,
+    square_part,
+    first_part,
+    second_part,
     chip_own,
     chip_all,
     square_own,
@@ -148,14 +151,6 @@
     for load in loads:
         load.start()
 
-    for load in loads[2:8]:
-        load.wait()
-    master_all[z, y, :, :kc] = master_key_v[...].astype(BF16)
-    master_all[z, y, :, kc:] = master_value_v[...].astype(BF16)
-    moments[0, z, y, :, :kc] = first_key[...].astype(BF16)
-    moments[0, z, y, :, kc:] = first_value[...].astype(BF16)
-    moments[1, z, y, :, :kc] = second_key[...].astype(BF16)
-    moments[1, z, y, :, kc:] = second_value[...].astype(BF16)
     loads[0].wait()
     loads[1].wait()
 
@@ -182,6 +177,14 @@
         own = basis_all.at[core, z, y]
         for k in FAR:
             send(own, own, basis_send.at[0], basis_one.at[k], fs=along(part, k))
+        for load in loads[2:8]:
+            load.wait()
+        master_all[z, y, :, :kc] = master_key_v[...].astype(BF16)
+        master_all[z, y, :, kc:] = master_value_v[...].astype(BF16)
+        moments[0, z, y, :, :kc] = first_key[...].astype(BF16)
+        moments[0, z, y, :, kc:] = first_value[...].astype(BF16)
+        moments[1, z, y, :, :kc] = second_key[...].astype(BF16)
+        moments[1, z, y, :, kc:] = second_value[...].astype(BF16)
         for k in FAR:
             for a, block in pack_arrays((z, y)):
                 send(block, block, pack_send.at[0, a], pack_one.at[a, k], fs=along(part, k))
@@ -305,20 +308,28 @@
     by_core(low_second)
     by_core(pack_far)
 
+    wait_recv(low_all.at[:, pl.ds(0, SIDE - 1)], low_recv.at[1])
+    for j in range(n):
+        at = slice(j * rank_rows, (j + 1) * rank_rows)
+        each = low_all[j // SIDE, j % SIDE].astype(F32)
+        low_part[at, :] = (1.0 - beta_first) * each
+        square_part[at, :] = (1.0 - beta_second) * each * each
+    by_core(functools.partial(pack_last, 0))
+    for j in range(n):
+        at = slice(j * rank_rows, (j + 1) * rank_rows)
+        first_part[at, :] = beta_first * moments[0, j // SIDE, j % SIDE].astype(F32)
+        second_part[at, :] = beta_second * moments[1, j // SIDE, j % SIDE].astype(F32)
+
     wait_recv(square_all.at[pl.ds(1, n - 1)], square_recv.at[0])
     total = square_own[...] + jnp.sum(square_all[1:], axis=0)
     grad_scale = (1.0 / jnp.sqrt(total / count + norm_eps))[0:1, 0:1]
     scaled_out[...] = low * grad_scale
-
-    by_core(functools.partial(pack_last, 0))
-    wait_recv(low_all.at[:, pl.ds(0, SIDE - 1)], low_recv.at[1])
-
-    for j in range(n):
-        scaled = low_all[j // SIDE, j % SIDE].astype(F32) * grad_scale
-        moved = beta_first * moments[0, j // SIDE, j % SIDE].astype(F32) + (1.0 - beta_first) * scaled
-        spread = beta_second * moments[1, j // SIDE, j % SIDE].astype(F32) + (1.0 - beta_second) * scaled * scaled
-        turned[j * rank_rows : (j + 1) * rank_rows, :] = moved / (jnp.sqrt(spread) + epsilon)
-    dirs[...] = turned[...].astype(BF16)
+    height = n * rank_rows // SIDE
+    for i in range(SIDE):
+        at = slice(i * height, (i + 1) * height)
+        moved = first_part[at, :] + grad_scale * low_part[at, :]
+        spread = second_part[at, :] + grad_scale * grad_scale * square_part[at, :]
+        dirs[at, :] = (moved / (jnp.sqrt(spread) + epsilon)).astype(BF16)
 
     by_core(functools.partial(pack_last, 1))
 
@@ -439,6 +450,9 @@
             pltpu.VMEM((rank_rows, cols), BF16),
             pltpu.VMEM((SIDE, SIDE, rank_rows, cols), BF16),
             pltpu.VMEM((rank, cols), F32),
+            pltpu.VMEM((rank, cols), F32),
+            pltpu.VMEM((rank, cols), F32),
+            pltpu.VMEM((rank, cols), F32),
             pltpu.VMEM(small, F32),
             pltpu.VMEM((tp, *small), F32),
             pltpu.VMEM(small, F32),

time: 51.9 us -> 51.9 us (level)
  no operation moved by 1% of the time
where the time goes in v5:
time: 51.9 us; the launch traced here: 51.7 us
  Pallas kernels  50.9 us (98%)
  between operations  0.76 us (1%)
    pallas_call x1, Pallas kernels, on_device(): pl.pallas_call(functools.partial(exchange_kernel, n, tp, rank * cols * tp...  49.1 us
    pallas_call x1, Pallas kernels, on_device(): pl.pallas_call(final_kernel, out_shape=(jax.ShapeDtypeStruct((d, kc), BF1...  1.87 us

profile of v5, /device:TPU:1, one launch (start us, length us, event | category | flops | bytes accessed | tf_op | source)
XLA Modules:
  0.0 51.7 jit_solution(877401158451375632)
XLA Ops:
  0.6 0.0 copy-start.4
  0.7 0.0 copy-start.3
  0.7 0.0 copy-start.6
  0.7 0.0 copy-start.5
  0.7 0.0 copy-start
  0.7 0.0 copy-start.2
  0.7 0.0 copy-start.1
  0.7 49.1 %shard_map.177 = (bf16[2,8,8,32,128]{4,3,2,1,0:T(8,128)(2,1)S(1)}, bf16[8,8,32,384]{3,2,1,0:T(8,128)(2,1)S(1)}, bf16[256,384]{1,0:T(8,128)(2,1)S(1)}, f32[4,384]{1,0:T(4,128)S(1)}) custom-call(bf16[1024,2048]{1,0:T(8,128)(2,1)} %normed.1, bf16[1024,128]{1,0:T(8,128)(2,1)} %key_cot.1, bf16[1024,256]{1,0:T(8,128)(2,1)} %value_cot.1, bf16[32,256]{1,0:T(8,128)(2,1)} %basis.1, ...), custom_call_target="tpu_custom_call" | custom-call | tf_op jit(solution)/shard_map/pallas_call | solution.py:425
  49.8 0.0 copy-done.4
  49.8 0.0 copy-done.3
  49.8 0.0 copy-done.6
  49.8 0.0 copy-done.5
  49.8 0.0 copy-done
  49.8 0.0 copy-done.2
  49.8 0.0 copy-done.1
  49.8 1.9 %shard_map.178 = (bf16[2048,128]{1,0:T(8,128)(2,1)}, bf16[2048,256]{1,0:T(8,128)(2,1)}, f32[32,128]{1,0:T(8,128)}, f32[32,256]{1,0:T(8,128)}, f32[32,128]{1,0:T(...) custom-call(bf16[2,8,8,32,128]{4,3,2,1,0:T(8,128)(2,1)S(1)} %get-tup, ...), custom_call_target="tpu_custom_call" | custom-call | tf_op jit(solution)/shard_map/pallas_call | solution.py:476
Async XLA Ops:
  0.6 49.1 %copy-start.4 = (f32[4,256]{1,0:T(4,128)S(1)}, f32[4,256]{1,0:T(4,128)}, u32[]{:S(2)}) copy-start(f32[4,256]{1,0:T(4,128)} %second_value.1) | copy-start | bytes 12292
  0.7 49.1 %copy-start.3 = (f32[4,256]{1,0:T(4,128)S(1)}, f32[4,256]{1,0:T(4,128)}, u32[]{:S(2)}) copy-start(f32[4,256]{1,0:T(4,128)} %first_value.1) | copy-start | bytes 12292
  0.7 49.1 %copy-start.6 = (f32[4,128]{1,0:T(4,128)S(1)}, f32[4,128]{1,0:T(4,128)}, u32[]{:S(2)}) copy-start(f32[4,128]{1,0:T(4,128)} %second_key.1) | copy-start | bytes 6148
  0.7 49.1 %copy-start.5 = (f32[4,128]{1,0:T(4,128)S(1)}, f32[4,128]{1,0:T(4,128)}, u32[]{:S(2)}) copy-start(f32[4,128]{1,0:T(4,128)} %first_key.1) | copy-start | bytes 6148
  0.7 49.1 %copy-start = (f32[32,256]{1,0:T(8,128)S(1)}, f32[32,256]{1,0:T(8,128)}, u32[]{:S(2)}) copy-start(f32[32,256]{1,0:T(8,128)} %master_value.3) | copy-start | bytes 98308
  0.7 49.1 %copy-start.2 = (f32[32,128]{1,0:T(8,128)S(1)}, f32[32,128]{1,0:T(8,128)}, u32[]{:S(2)}) copy-start(f32[32,128]{1,0:T(8,128)} %master_key.3) | copy-start | bytes 49156
  0.7 49.1 %copy-start.1 = (bf16[32,256]{1,0:T(8,128)(2,1)S(1)}, bf16[32,256]{1,0:T(8,128)(2,1)}, u32[]{:S(2)}) copy-start(bf16[32,256]{1,0:T(8,128)(2,1)} %basis.1) | copy-start | bytes 49156
